TPU v7x, 256 devices: a 4x2x16 block of a 4x16x16 slice. The times are simulated.
256 devices in a mesh: grp: 2 (over y), sp: 16 (over z), tp: 8 (over x, core).
Axes of the slice: x: 4, y: 2, z: 16, core: 2. Of those that a mesh axis runs over, the one named last changes fastest.
The devices are a block of a 4x16x16 slice.
Arguments:
- queries: bfloat16 [24576, 1024], P(('grp', 'sp'), 'tp'), parts along dimension 0, may hold values from -200 to 200
- key_rows: bfloat16 [24576, 512], P(('grp', 'sp'), 'tp'), parts along dimension 0, may hold values from -6 to 6
- value_rows: bfloat16 [24576, 512], P(('grp', 'sp'), 'tp'), parts along dimension 0, may hold values from -6 to 6
- doc_ids: int32 [24576], P(('grp', 'sp')), parts along dimension 0, may hold values from 0 to 7, never falling along the last dimension, each value on 1 to 3072 neighbouring positions
- sink_logits: float32 [16], P('tp'), may hold values from 2 to 7
- out_weight: bfloat16 [1024, 2048], P('tp', 'sp'), may hold values from -0.1875 to 0.1875
- residual: bfloat16 [24576, 2048], P(('grp', 'sp', 'tp')), parts along dimension 0, may hold values from -6 to 6
- gain_mixed: float32 [2048], replicated, may hold values from 0.1 to 1.9
- gain_before: float32 [2048], replicated, may hold values from 0.1 to 1.9
- gain_after: float32 [2048], replicated, may hold values from 0.1 to 1.9
- gate_weight: bfloat16 [2048, 6144], P('sp', 'tp'), may hold values from -0.125 to 0.125
- up_weight: bfloat16 [2048, 6144], P('sp', 'tp'), may hold values from -0.125 to 0.125
- down_weight: bfloat16 [6144, 2048], P('tp', 'sp'), may hold values from -0.078125 to 0.078125
Outputs:
- layer_out: bfloat16 [24576, 2048], P(('grp', 'sp', 'tp')), parts along dimension 0
There are 2 independent parts, one for each index of `grp`. A program takes and returns all parts, laid end to end along the dimension named above; an argument that names none is the same for every part. Nothing has to cross between parts.
All inputs are finite; a program needn't handle non-finite values.
Results may differ from a plain program's by a relative error of at most 0.015.
Values may be sent and summed in bfloat16 or wider, within the bound.
A program may use at most 128 MiB of HBM per device.

v0:
```python
import jax
import jax.numpy as jnp
from jax import lax
from jax.sharding import PartitionSpec as P

HEAD_DIM = 64
WINDOW = 128


epsilon = 1e-06
masked_value = -1e30


def passed_along(value, axis, steps):
    count = lax.axis_size(axis)
    first, last = (max(0, -steps), min(count, count - steps))
    return lax.ppermute(value, axis, [(source, source + steps) for source in range(first, last)])


def from_everyone(shard, axis):
    size = lax.axis_size(axis)
    return lax.all_to_all(
        jnp.broadcast_to(shard[None], (size, *shard.shape)), axis, 0, 0, tiled=True
    )


def laid_out(pieces, dim):
    pieces = jnp.moveaxis(pieces, 0, dim)
    lengths = pieces.shape
    return pieces.reshape(*lengths[:dim], lengths[dim] * lengths[dim + 1], *lengths[dim + 2 :])


def gather_directly(shard, axis, dim):
    pieces = from_everyone(shard, axis)
    return laid_out(pieces, dim)


def turned_gather(arrays, axis, dims):
    turned = [jnp.moveaxis(a, dim, 0) for a, dim in zip(arrays, dims)]
    both = jnp.concatenate([t.reshape(len(t), -1) for t in turned], axis=1)
    filled, at, finished = (lax.all_gather(both, axis, axis=0, tiled=True), 0, [])
    for t, dim in zip(turned, dims):
        piece = filled[:, at : at + t[0].size].reshape(-1, *t.shape[1:])
        finished.append(jnp.moveaxis(piece, 0, dim))
        at += t[0].size
    return tuple(finished)


def split_up(shard, dim, size):
    lengths = shard.shape
    pieces = shard.reshape(*lengths[:dim], size, lengths[dim] // size, *lengths[dim + 1 :])
    return jnp.moveaxis(pieces, dim, 0)


def summed_on_arrival(shard, axis, dim):
    size = lax.axis_size(axis)
    pieces = lax.all_to_all(split_up(shard, dim, size), axis, 0, 0, tiled=True)
    return jnp.sum(pieces.astype(jnp.float32), axis=0)


def stored(value):
    return lax.optimization_barrier(value.astype(jnp.bfloat16)).astype(jnp.float32)


def rms_scaled(value, gain):
    return value * lax.rsqrt(jnp.mean(value * value, axis=-1, keepdims=True) + epsilon) * gain


def windows(array, blocks):
    first = array[:-WINDOW].reshape((blocks, WINDOW) + array.shape[1:])
    second = array[WINDOW:].reshape((blocks, WINDOW) + array.shape[1:])
    return jnp.concatenate([first, second], axis=1)


def attend(queries, key_rows, value_rows, doc_ids, sink_logits):
    length = queries.shape[0]
    blocks = length // WINDOW
    local_kv = key_rows.shape[1] // HEAD_DIM
    group_size = queries.shape[1] // HEAD_DIM // local_kv
    offset = lax.axis_index("sp") * length
    tail_keys, tail_values, tail_docs = passed_along(
        (key_rows[length - WINDOW :], value_rows[length - WINDOW :], doc_ids[length - WINDOW :]),
        "sp",
        1,
    )
    key_blocks = windows(jnp.concatenate([tail_keys, key_rows], axis=0), blocks).reshape(
        blocks, 2 * WINDOW, local_kv, HEAD_DIM
    )
    value_blocks = windows(jnp.concatenate([tail_values, value_rows], axis=0), blocks).reshape(
        blocks, 2 * WINDOW, local_kv, HEAD_DIM
    )
    key_docs = windows(jnp.concatenate([tail_docs, doc_ids], axis=0), blocks)
    key_places = windows(offset - WINDOW + jnp.arange(length + WINDOW, dtype=jnp.int32), blocks)
    query_places = (offset + jnp.arange(length, dtype=jnp.int32)).reshape(blocks, WINDOW)
    query_docs = doc_ids.reshape(blocks, WINDOW)
    query_blocks = queries.reshape(blocks, WINDOW, local_kv, group_size, HEAD_DIM)
    scores = jnp.einsum(
        "bqhgd,bkhd->bhgqk", query_blocks, key_blocks, preferred_element_type=jnp.float32
    ) * HEAD_DIM ** (-0.5)
    distance = query_places[:, :, None] - key_places[:, None, :]
    valid = (distance >= 0) & (distance < WINDOW) & (key_places[:, None, :] >= 0)
    valid = valid & (query_docs[:, :, None] == key_docs[:, None, :])
    scores = jnp.where(valid[:, None, None], scores, masked_value)
    sinks = sink_logits.reshape(local_kv, group_size)[None, :, :, None]
    top = jnp.maximum(jnp.max(scores, axis=-1), sinks)
    weight = jnp.exp(scores - top[..., None])
    denom = jnp.sum(weight, axis=-1) + jnp.exp(sinks - top)
    summed = jnp.einsum(
        "bhgqk,bkhd->bqhgd",
        weight.astype(jnp.bfloat16),
        value_blocks,
        preferred_element_type=jnp.float32,
    )
    scale = jnp.transpose(denom, (0, 3, 1, 2))[..., None]
    return (summed / scale).reshape(length, queries.shape[1]).astype(jnp.bfloat16)


def per_device(
    queries,
    key_rows,
    value_rows,
    doc_ids,
    sink_logits,
    out_weight,
    residual,
    gain_mixed,
    gain_before,
    gain_after,
    gate_weight,
    up_weight,
    down_weight,
):
    mixed = attend(queries, key_rows, value_rows, doc_ids, sink_logits)
    head_columns = gather_directly(out_weight, "sp", 1)
    by_rows = lax.all_to_all(mixed, "tp", split_axis=0, concat_axis=1, tiled=True)
    projected = jnp.dot(
        by_rows,
        lax.all_gather(head_columns, "tp", axis=0, tiled=True),
        preferred_element_type=jnp.float32,
    )
    projected = stored(projected)
    after = stored(residual.astype(jnp.float32) + rms_scaled(projected, gain_mixed))
    normed = rms_scaled(after, gain_before).astype(jnp.bfloat16)
    full_gate, full_up, full_down = turned_gather(
        (gate_weight, up_weight, down_weight), "sp", (0, 0, 1)
    )
    piece = lax.all_gather(normed, "tp", axis=0, tiled=True)
    gate = jnp.dot(piece, full_gate, preferred_element_type=jnp.float32)
    upward = jnp.dot(piece, full_up, preferred_element_type=jnp.float32)
    hidden = (jax.nn.silu(gate) * upward).astype(jnp.bfloat16)
    ffn_out = stored(
        summed_on_arrival(
            jnp.dot(hidden, full_down, preferred_element_type=jnp.float32).astype(jnp.bfloat16),
            "tp",
            0,
        )
    )
    return (after + 0.5 * rms_scaled(ffn_out, gain_after)).astype(jnp.bfloat16)


def solution(mesh):
    return jax.shard_map(
        per_device,
        mesh=mesh,
        in_specs=(
            P(("grp", "sp"), "tp"),
            P(("grp", "sp"), "tp"),
            P(("grp", "sp"), "tp"),
            P(("grp", "sp")),
            P("tp"),
            P("tp", "sp"),
            P(("grp", "sp", "tp"), None),
            P(),
            P(),
            P(),
            P("sp", "tp"),
            P("sp", "tp"),
            P("tp", "sp"),
        ),
        out_specs=P(("grp", "sp", "tp"), None),
        check_vma=False,
    )
```

profile of v0, /device:TPU:33, one launch (start us, length us, event | category | flops | bytes accessed | tf_op | source)
XLA Modules:
  0.0 348.9 jit_solution(4281266326615611289)
XLA Ops:
  6.5 0.0 copy-start.7
  6.5 0.0 copy-start.1
  6.6 0.0 copy-start
  6.6 0.1 all-gather.4.cloned.1.call-start
  6.6 1.0 copy.40
  7.6 0.1 broadcast_in_dim.16
  7.7 47.2 %all_to_all.26 = bf16[16,128,128]{1,2,0:T(8,128)(2,1)} all-to-all(bf16[16,128,128]{1,2,0:T(8,128)(2,1)S(1)} %broadcast_in_dim.16), channel_id=1, replica_groups=mesh['grp'=2,'sp'=16,'tp'=8] {'sp'}, dimensions={0} | all-to-all | bytes 1048576 | tf_op jit(solution)/shard_map/all_to_all | solution.py:22
  54.9 0.1 all-gather.4.cloned.1.call-update
  54.9 0.1 all-gather.6.cloned.1.call-start
  55.0 0.7 slice.49
  55.7 5.3 %collective-permute-start.1 = (s32[128]{0:T(128)S(1)}, s32[128]{0:T(128)S(1)}, u32[]{:S(2)}, u32[]{:S(2)}) collective-permute-start(s32[128]{0:T(128)S(1)} %slice.49), channel_id=1, source_target_pairs={{0,8},{8,16},{16,24},{24,32},{32,40},{40,48},{48,56},{56,64},{64,7... | collective-permute-start | bytes 1544 | tf_op jit(solution)/shard_map/ppermute | solution.py:17
  61.0 0.7 slice.45
  61.7 2.2 collective-permute-start
  63.9 0.7 slice.52
  64.6 4.6 %collective-permute-start.2 = (bf16[128,64]{0,1:T(8,128)(2,1)S(1)}, bf16[128,64]{0,1:T(8,128)(2,1)S(1)}, u32[]{:S(2)}, u32[]{:S(2)}) collective-permute-start(bf16[128,64]{0,1:T(8,128)(2,1)S(1)} %slice.52), channel_id=1, source_target_pairs={{0,8},{8,16},{16,24},{24,32},{32,40},{40,48},{48,56},{56,64},{64,7... | collective-permute-start | bytes 49160 | tf_op jit(solution)/shard_map/ppermute | solution.py:17
  69.2 0.0 copy-done
  69.3 0.0 copy-done.1
  69.3 0.0 copy-done.6
  69.3 0.2 reshape.170
  69.5 0.0 collective-permute-done.1
  69.5 0.0 copy-done.7
  69.6 1.0 fusion.30
  70.6 0.0 collective-permute-done.2
  70.6 0.0 collective-permute-done
  70.6 0.5 fusion.48
  71.1 0.0 copy-done.11
  71.1 0.1 broadcast_maximum_fusion
  71.2 0.2 fusion.7
  71.4 0.1 fusion.43
  71.5 0.4 fusion.13
  71.9 0.4 copy.48
  72.3 0.2 reshape.171
  72.5 17.5 %all_to_all.27 = bf16[8,96,128]{2,1,0:T(8,128)(2,1)S(1)} all-to-all(bf16[8,96,128]{2,1,0:T(8,128)(2,1)S(1)} %reshape.171), channel_id=1, replica_groups=mesh['grp'=2,'sp'=16,'tp'=8] {'tp'}, dimensions={0} | all-to-all | bytes 393216 | tf_op jit(solution)/shard_map/all_to_all | solution.py:135
  90.0 12.1 %all-gather.4.cloned.1.call-done = bf16[1024,2048]{0,1:T(8,128)(2,1)} async-done(((bf16[128,2048]{0,1:T(8,128)(2,1)}), bf16[1024,2048]{0,1:T(8,128)(2,1)}) %all-gather.4.cloned.1.call-update) | async-done | bytes 4194320 | tf_op jit(solution)/shard_map/all_gather | solution.py:138
  102.2 3.6 %convolution_convert_fusion.1 = bf16[96,2048]{1,0:T(8,128)(2,1)S(1)} fusion(bf16[1024,2048]{0,1:T(8,128)(2,1)} %all-gather.4.cloned.1.call-done, bf16[8,96,128]{2,1,0:T(8,128)(2,1)S(1)} %all_to_all.27), kind=kOutput, calls=%fused_computation.7 | convolution fusion | flops 402849792 | bytes 4784128 | tf_op jit(solution)/shard_map/dot_general | solution.py:136
  105.8 0.0 copy-start.4
  105.8 0.0 copy-start.5
  105.8 0.0 copy-start.3
  105.8 0.2 fusion.14
  106.0 0.0 copy-done.2
  106.0 0.0 copy-done.8
  106.0 0.2 fusion.17
  106.2 0.2 fusion.21
  106.4 0.0 copy-done.9
  106.4 0.9 fusion.23
  107.3 0.1 all-gather.6.cloned.1.call-update
  107.4 0.2 all-gather.8.cloned.1.call-start
  107.6 0.0 copy-done.4
  107.6 0.2 copy.41
  107.8 0.0 copy-done.5
  107.8 0.2 copy.42
  108.0 0.0 copy-done.3
  108.0 0.9 pad_maximum_fusion
  108.9 0.1 all-gather.8.cloned.1.call-update
  108.9 31.3 %all-gather.6.cloned.1.call-done = bf16[768,2048]{1,0:T(8,128)(2,1)} async-done(((bf16[96,2048]{1,0:T(8,128)(2,1)}), bf16[768,2048]{1,0:T(8,128)(2,1)}) %all-gather.6.cloned.1.call-update) | async-done | bytes 3145744 | tf_op jit(solution)/shard_map/all_gather | solution.py:147
  140.2 128.3 %all-gather.8.cloned.1.call-done = bf16[2048,2304]{0,1:T(8,128)(2,1)} async-done(((bf16[128,2304]{0,1:T(8,128)(2,1)}), bf16[2048,2304]{0,1:T(8,128)(2,1)}) %all-gather.8.cloned.1.call-update) | async-done | bytes 9437200 | tf_op jit(solution)/shard_map/all_gather | solution.py:41
  268.5 6.9 %fusion.3 = f32[768,768]{1,0:T(8,128)} fusion(bf16[768,2048]{1,0:T(8,128)(2,1)} %all-gather.6.cloned.1.call-done, bf16[2048,2304]{0,1:T(8,128)(2,1)} %all-gather.8.cloned.1.call-done), kind=kOutput, calls=%fused_computation.4 | convolution fusion | flops 2415919104 | bytes 8650752 | tf_op jit(solution)/shard_map/dot_general | solution.py:148
  275.4 0.0 copy-done.12
  275.4 11.0 %convolution_convert_fusion = bf16[768,2048]{1,0:T(8,128)(2,1)} fusion(bf16[2048,2304]{0,1:T(8,128)(2,1)} %all-gather.8.cloned.1.call-done, f32[768,768]{1,0:T(8,128)} %fusion.3, bf16[768,2048]{1,0:T(8,128)(2,1)S(1)} %copy-done.12), kind=kOutput, calls=%fused_computation | convolution fusion | flops 4836950016 | bytes 14942208 | tf_op jit(solution)/shard_map/dot_general | solution.py:153
  286.4 51.4 %all_to_all.28 = bf16[8,96,2048]{2,1,0:T(8,128)(2,1)S(1)} all-to-all(bf16[8,96,2048]{2,1,0:T(8,128)(2,1)} %bitcast.84), channel_id=1, replica_groups=mesh['grp'=2,'sp'=16,'tp'=8] {'tp'}, dimensions={0} | all-to-all | bytes 6291456 | tf_op jit(solution)/shard_map/all_to_all | solution.py:57
  337.7 1.4 reduce_sum.54
  339.2 1.2 fusion.18
  340.3 0.0 copy-done.10
  340.4 2.0 fusion.24
  (21 shorter events, 0.2 us)
Async XLA Ops:
  6.5 63.0 %copy-start.7 = (s32[768]{0:T(1024)S(1)}, s32[768]{0:T(1024)}, u32[]{:S(2)}) copy-start(s32[768]{0:T(1024)} %param.16) | copy-start | bytes 9220
  6.5 62.7 %copy-start.1 = (bf16[768,64]{0,1:T(8,128)(2,1)S(1)}, bf16[768,64]{0,1:T(8,128)(2,1)}, u32[]{:S(2)}) copy-start(bf16[768,64]{0,1:T(8,128)(2,1)} %param.15) | copy-start | bytes 294916
  6.6 62.7 %copy-start = (bf16[768,64]{0,1:T(8,128)(2,1)S(1)}, bf16[768,64]{0,1:T(8,128)(2,1)}, u32[]{:S(2)}) copy-start(bf16[768,64]{0,1:T(8,128)(2,1)} %param.14) | copy-start | bytes 294916
  6.6 62.8 %copy-start.6 = (bf16[768,128]{1,0:T(8,128)(2,1)S(1)}, bf16[768,128]{1,0:T(8,128)(2,1)}, u32[]{:S(2)}) copy-start(bf16[768,128]{1,0:T(8,128)(2,1)} %param.13) | copy-start | bytes 589828
  6.6 95.6 %all-gather.4.cloned.1.call-start = ((), (), s32[]{:S(2)}) async-start(), calls=%async_computation.3 | async-start | bytes 4718592 | tf_op jit(solution)/shard_map/all_gather | solution.py:138
  54.9 16.2 %copy-start.11 = (f32[2]{0:T(128)S(1)}, f32[2]{0:T(128)}, u32[]{:S(2)}) copy-start(f32[2]{0:T(128)} %param.17) | copy-start | bytes 28
  54.9 85.2 %all-gather.6.cloned.1.call-start = ((), (), s32[]{:S(2)}) async-start(), calls=%async_computation.4 | async-start | bytes 3538944 | tf_op jit(solution)/shard_map/all_gather | solution.py:147
  55.7 13.8 %collective-permute-start.1 = (s32[128]{0:T(128)S(1)}, s32[128]{0:T(128)S(1)}, u32[]{:S(2)}, u32[]{:S(2)}) collective-permute-start(s32[128]{0:T(128)S(1)} %slice.49), channel_id=1, source_target_pairs={{0,8},{8,16},{16,24},{24,32},{32,40},{40,48},{48,56},{56,64},{64,7... | collective-permute-start | bytes 1544 | tf_op jit(solution)/shard_map/ppermute | solution.py:17
  61.7 8.9 %collective-permute-start = (bf16[128,64]{0,1:T(8,128)(2,1)S(1)}, bf16[128,64]{0,1:T(8,128)(2,1)S(1)}, u32[]{:S(2)}, u32[]{:S(2)}) collective-permute-start(bf16[128,64]{0,1:T(8,128)(2,1)S(1)} %slice.45), channel_id=1, source_target_pairs={{0,8},{8,16},{16,24},{24,32},{32,40},{40,48},{48,56},{56,64},{64,7... | collective-permute-start | bytes 49160 | tf_op jit(solution)/shard_map/ppermute | solution.py:17
  64.6 5.9 %collective-permute-start.2 = (bf16[128,64]{0,1:T(8,128)(2,1)S(1)}, bf16[128,64]{0,1:T(8,128)(2,1)S(1)}, u32[]{:S(2)}, u32[]{:S(2)}) collective-permute-start(bf16[128,64]{0,1:T(8,128)(2,1)S(1)} %slice.52), channel_id=1, source_target_pairs={{0,8},{8,16},{16,24},{24,32},{32,40},{40,48},{48,56},{56,64},{64,7... | collective-permute-start | bytes 49160 | tf_op jit(solution)/shard_map/ppermute | solution.py:17
  90.0 16.0 %copy-start.2 = (bf16[96,2048]{1,0:T(8,128)(2,1)S(1)}, bf16[96,2048]{1,0:T(8,128)(2,1)}, u32[]{:S(2)}) copy-start(bf16[96,2048]{1,0:T(8,128)(2,1)} %param.19) | copy-start | bytes 1179652
  90.0 16.0 %copy-start.8 = (f32[2048]{0:T(1024)S(1)}, f32[2048]{0:T(1024)}, u32[]{:S(2)}) copy-start(f32[2048]{0:T(1024)} %param.20) | copy-start | bytes 24580
  90.0 16.4 %copy-start.9 = (f32[2048]{0:T(1024)S(1)}, f32[2048]{0:T(1024)}, u32[]{:S(2)}) copy-start(f32[2048]{0:T(1024)} %param.21) | copy-start | bytes 24580
  105.8 1.9 copy-start.4
  105.8 2.0 copy-start.5
  105.8 2.2 copy-start.3
  107.4 161.1 %all-gather.8.cloned.1.call-start = ((), (), s32[]{:S(2)}) async-start(), calls=%async_computation.5 | async-start | bytes 10027008 | tf_op jit(solution)/shard_map/all_gather | solution.py:41
  140.2 135.2 %copy-start.12 = (bf16[768,2048]{1,0:T(8,128)(2,1)S(1)}, bf16[768,2048]{1,0:T(8,128)(2,1)}, u32[]{:S(2)}) copy-start(bf16[768,2048]{1,0:T(8,128)(2,1)} %all-gather.6.cloned.1.call-done) | copy-start | bytes 9437188
  337.7 2.6 copy-start.10
Sparse Core Ops, SparseCore 0:
  55.1 47.0 all-gather.3
  107.5 32.6 all-gather.5
  141.9 126.5 all-gather.7
where the time goes:
time: 349 us
  waiting for transfers between devices  172 us (49%)
  blocking collectives  116 us (33%)
  matrix products  22.3 us (6%)
  between operations  13.5 us (4%)
  starting transfers between devices  12.4 us (4%)
  other arithmetic  8.34 us (2%)
  local copies, waits for them, and re-layouts  4.39 us (1%)
    all_gather x1, waiting for transfers between devices, turned_gather(): lax.all_gather(both, axis, axis=0, tiled=True)  128 us
    all_to_all x1, blocking collectives, summed_on_arrival(): pieces = lax.all_to_all(split_up(shard, dim, size), axis, 0, 0, tiled=True)  51.4 us
    all_to_all x1, blocking collectives, from_everyone(): lax.all_to_all(jnp.broadcast_to(shard[None], (size, *shard.shape)), axis,...  47.2 us
    all_gather x1, waiting for transfers between devices, per_device(): piece = lax.all_gather(normed, 'tp', axis=0, tiled=True)  31.3 us
    all_to_all x1, blocking collectives, per_device(): lax.all_to_all(mixed, 'tp', split_axis=0, concat_axis=1, tiled=True)  17.5 us
    all_gather x1, waiting for transfers between devices, per_device(): lax.all_gather(head_columns, 'tp', axis=0, tiled=True)  12.1 us
    ppermute x3, starting transfers between devices, passed_along(): lax.ppermute(value, axis, [(source, source + steps) for source in range(f...  12 us
    dot_general x1, matrix products, per_device(): jnp.dot(hidden, full_down, preferred_element_type=jnp.float32)  11 us
  transfers between devices with their start and end apart: 6, of which 3 were waited for; matrix products, arithmetic and copies ran while one was open for 2% of the time, Pallas kernels for 0%

commit v1 on v0

--- a/solution.py
+++ b/solution.py
@@ -1,61 +1,27 @@
+import functools
+
 import jax
 import jax.numpy as jnp
 from jax import lax
+from jax.experimental import pallas as pl
+from jax.experimental.pallas import tpu as pltpu
 from jax.sharding import PartitionSpec as P
 
 HEAD_DIM = 64
 WINDOW = 128
-
-
 epsilon = 1e-06
 masked_value = -1e30
+MESH = pl.DeviceIdType.MESH
+f32 = jnp.float32
+bf16 = jnp.bfloat16
+
+HALVES = 2
 
 
 def passed_along(value, axis, steps):
     count = lax.axis_size(axis)
     first, last = (max(0, -steps), min(count, count - steps))
     return lax.ppermute(value, axis, [(source, source + steps) for source in range(first, last)])
-
-
-def from_everyone(shard, axis):
-    size = lax.axis_size(axis)
-    return lax.all_to_all(
-        jnp.broadcast_to(shard[None], (size, *shard.shape)), axis, 0, 0, tiled=True
-    )
-
-
-def laid_out(pieces, dim):
-    pieces = jnp.moveaxis(pieces, 0, dim)
-    lengths = pieces.shape
-    return pieces.reshape(*lengths[:dim], lengths[dim] * lengths[dim + 1], *lengths[dim + 2 :])
-
-
-def gather_directly(shard, axis, dim):
-    pieces = from_everyone(shard, axis)
-    return laid_out(pieces, dim)
-
-
-def turned_gather(arrays, axis, dims):
-    turned = [jnp.moveaxis(a, dim, 0) for a, dim in zip(arrays, dims)]
-    both = jnp.concatenate([t.reshape(len(t), -1) for t in turned], axis=1)
-    filled, at, finished = (lax.all_gather(both, axis, axis=0, tiled=True), 0, [])
-    for t, dim in zip(turned, dims):
-        piece = filled[:, at : at + t[0].size].reshape(-1, *t.shape[1:])
-        finished.append(jnp.moveaxis(piece, 0, dim))
-        at += t[0].size
-    return tuple(finished)
-
-
-def split_up(shard, dim, size):
-    lengths = shard.shape
-    pieces = shard.reshape(*lengths[:dim], size, lengths[dim] // size, *lengths[dim + 1 :])
-    return jnp.moveaxis(pieces, dim, 0)
-
-
-def summed_on_arrival(shard, axis, dim):
-    size = lax.axis_size(axis)
-    pieces = lax.all_to_all(split_up(shard, dim, size), axis, 0, 0, tiled=True)
-    return jnp.sum(pieces.astype(jnp.float32), axis=0)
 
 
 def stored(value):
@@ -113,6 +79,386 @@
     )
     scale = jnp.transpose(denom, (0, 3, 1, 2))[..., None]
     return (summed / scale).reshape(length, queries.shape[1]).astype(jnp.bfloat16)
+
+
+def kernel(
+    normed_ref,
+    after_ref,
+    gate_ref,
+    up_ref,
+    down_ref,
+    gain_ref,
+    out_ref,
+    gfull,
+    ufull,
+    dfull,
+    xn,
+    hid,
+    pcs,
+    pcr,
+    keep,
+    raws,
+    rawr,
+    nbs,
+    nbr,
+    own_acc,
+    ffn,
+    z_send,
+    z_recv,
+    y_send,
+    y_recv,
+    ag_send,
+    ag_recv,
+    pc_send,
+    pc_recv,
+    raw_send,
+    raw_recv,
+    nb_send,
+    nb_recv,
+):
+    N_SP, N_TP = lax.axis_size("sp"), lax.axis_size("tp")
+    N_X, REACH = N_TP // 2, N_SP // 2
+    g = lax.axis_index("grp")
+    s = lax.axis_index("sp")
+    t = lax.axis_index("tp")
+    core = lax.rem(t, 2)
+    x = t // 2
+    rows = normed_ref.shape[0]
+    half = N_X * rows
+    depth = gate_ref.shape[0]
+    third = gate_ref.shape[1] // 3
+    width = down_ref.shape[1]
+
+    z_next = {"sp": lax.rem(s + 1, N_SP)}
+    z_prev = {"sp": lax.rem(s + N_SP - 1, N_SP)}
+    z_to = (z_next, z_prev)
+    x_next = {"tp": lax.rem(t + 2, N_TP)}
+    x_prev = {"tp": lax.rem(t + N_TP - 2, N_TP)}
+    partner = {"tp": t + 1 - 2 * core}
+    odd = lax.rem(g, 2)
+    y_pair = {"grp": g + 1 - 2 * odd}
+    mine, theirs = 2 * odd, 2 - 2 * odd
+
+    barrier = pltpu.get_barrier_semaphore()
+    for device in (z_next, z_prev, x_next, x_prev, partner, y_pair):
+        pl.semaphore_signal(barrier, inc=1, device_id=device, device_id_type=MESH)
+    pl.semaphore_wait(barrier, 6)
+
+    pending = []
+
+    def send(src, dst, ssem, rsem, device):
+        copy = pltpu.make_async_remote_copy(
+            src_ref=src, dst_ref=dst, send_sem=ssem, recv_sem=rsem, device_id=device, device_id_type=MESH
+        )
+        copy.start()
+        pending.append(copy)
+
+    def landed(dst, ssem, rsem, device):
+        pltpu.make_async_remote_copy(
+            src_ref=dst, dst_ref=dst, send_sem=ssem, recv_sem=rsem, device_id=device, device_id_type=MESH
+        ).wait_recv()
+
+    fulls = (gfull, ufull)
+    owns = (gate_ref, up_ref)
+
+    def place(p, j, way, part, h):
+        if p < 2:
+            origin = lax.rem(s + N_SP - j, N_SP) if way == 0 else lax.rem(s + j, N_SP)
+            size = depth // HALVES
+            at = pl.multiple_of(origin * depth + h * size, size)
+            return fulls[p].at[part, pl.ds(at, size), :]
+        slot, side = (0, 1) if j == REACH else (j, way)
+        size = third // HALVES
+        at = pl.multiple_of(part * third + h * size, size)
+        return dfull.at[slot, side, pl.ds(at, size), :]
+
+    def dest(p, j, way, part, h):
+        if p < 2:
+            return place(p, j, way, part, h)
+        return place(p, j + 1, way, part, h)
+
+    def own_piece(p, part, h):
+        if p < 2:
+            size = depth // HALVES
+            return owns[p].at[pl.ds(h * size, size), pl.ds(pl.multiple_of(part * third, third), third)]
+        size = third // HALVES
+        return down_ref.at[pl.ds(pl.multiple_of(part * third + h * size, size), size), :]
+
+    def zi(p, j, way, kind, h):
+        return (((p * REACH + j) * 2 + way) * 2 + kind) * HALVES + h
+
+    def yi(p, j, way, h):
+        return ((p * REACH + j - 1) * 2 + way) * HALVES + h
+
+    def travels(j, way, kind):
+        return j < REACH - 1 or (j == REACH - 1 and way == kind)
+
+    def parts(kind):
+        return mine if kind == 0 else 1
+
+    def start_own(p):
+        for kind in range(2):
+            for h in range(HALVES):
+                for way in range(2):
+                    i = zi(p, 0, way, kind, h)
+                    send(
+                        own_piece(p, parts(kind), h),
+                        dest(p, 0, way, parts(kind), h),
+                        z_send.at[i],
+                        z_recv.at[i],
+                        z_to[way],
+                    )
+
+    def step(pieces, j):
+        for kind in range(2):
+            for p in pieces:
+                for h in range(HALVES):
+                    for way in range(2):
+                        if not travels(j - 1, way, kind):
+                            continue
+                        here = place(p, j, way, parts(kind), h)
+                        i = zi(p, j - 1, way, kind, h)
+                        landed(here, z_send.at[i], z_recv.at[i], z_to[1 - way])
+                        if j < REACH and travels(j, way, kind):
+                            k = zi(p, j, way, kind, h)
+                            send(here, dest(p, j, way, parts(kind), h), z_send.at[k], z_recv.at[k], z_to[way])
+                        if kind == 0:
+                            k = yi(p, j, way, h)
+                            send(here, here, y_send.at[k], y_recv.at[k], y_pair)
+
+    def swapped(p, j):
+        for way in range(2):
+            if not travels(j - 1, way, 0):
+                continue
+            for h in range(HALVES):
+                k = yi(p, j, way, h)
+                landed(place(p, j, way, theirs, h), y_send.at[k], y_recv.at[k], y_pair)
+
+    def block_of(c, xx):
+        return pl.multiple_of((c * N_X + lax.rem(xx + N_X, N_X)) * rows, rows)
+
+    start_own(0)
+    start_own(1)
+
+    h_rows = rows // 2
+    ag_i = [0]
+
+    def ag(src, dst, device):
+        i = ag_i[0]
+        ag_i[0] += 1
+        send(src, dst, ag_send.at[i], ag_recv.at[i], device)
+
+    def ag_wait(dst, i):
+        landed(dst, ag_send.at[i], ag_recv.at[i], partner)
+
+    own_rows = xn.at[pl.ds(block_of(core, x), rows), :]
+    ag(normed_ref, own_rows, x_next)
+    ag(normed_ref, own_rows, x_prev)
+    ag(normed_ref, own_rows, partner)
+    own_rows[...] = normed_ref[...]
+    for p in range(2):
+        at = pl.multiple_of(s * depth, depth)
+        for k in range(3):
+            fulls[p][k, pl.ds(at, depth), :] = owns[p][:, k * third : (k + 1) * third]
+    dfull[0, 0] = down_ref[...]
+
+    step((0, 1), 1)
+    from_prev = xn.at[pl.ds(block_of(core, x - 1), rows), :]
+    from_next = xn.at[pl.ds(block_of(core, x + 1), rows), :]
+    far_low = xn.at[pl.ds(block_of(core, x + 2), h_rows), :]
+    far_high = xn.at[pl.ds(pl.multiple_of(block_of(core, x + 2) + h_rows, h_rows), h_rows), :]
+    ag_wait(from_prev, 0)
+    low = xn.at[pl.ds(block_of(core, x - 1), h_rows), :]
+    ag(low, low, x_next)
+    ag(from_prev, from_prev, partner)
+    ag_wait(from_next, 1)
+    high = xn.at[pl.ds(pl.multiple_of(block_of(core, x + 1) + h_rows, h_rows), h_rows), :]
+    ag(high, high, x_prev)
+    ag(from_next, from_next, partner)
+    step((0, 1), 2)
+    ag_wait(far_low, 3)
+    ag(far_low, far_low, partner)
+    ag_wait(far_high, 5)
+    ag(far_high, far_high, partner)
+    step((0, 1), 3)
+    other = 1 - core
+    ag_wait(xn.at[pl.ds(block_of(other, x), rows), :], 2)
+    ag_wait(xn.at[pl.ds(block_of(other, x - 1), rows), :], 4)
+    ag_wait(xn.at[pl.ds(block_of(other, x + 1), rows), :], 6)
+    ag_wait(xn.at[pl.ds(block_of(other, x + 2), h_rows), :], 7)
+    ag_wait(xn.at[pl.ds(pl.multiple_of(block_of(other, x + 2) + h_rows, h_rows), h_rows), :], 8)
+
+    for j in range(4, REACH + 1):
+        step((0, 1), j)
+        if j == 6:
+            start_own(2)
+    for p in range(2):
+        for j in range(1, REACH + 1):
+            swapped(p, j)
+
+    done_down = 0
+    for k in range(3):
+        for b in range(2):
+            piece = xn[b * half : (b + 1) * half, :]
+            gate = jnp.dot(piece, gfull[k], preferred_element_type=f32)
+            up = jnp.dot(piece, ufull[k], preferred_element_type=f32)
+            hid[k, b * half : (b + 1) * half, :] = (gate / (1.0 + jnp.exp(-gate)) * up).astype(bf16)
+            done_down += 1
+            step((2,), done_down)
+
+    order = [*range(1, REACH), 0]
+    ways = ((x_next, x_prev), (x_prev, x_next))
+
+    def product(slot, at):
+        total = None
+        for k in range(3):
+            right = jnp.concatenate(
+                [dfull[slot, side, k * third : (k + 1) * third, :] for side in range(2)], axis=1
+            )
+            term = jnp.dot(hid[k, pl.ds(at, half), :], right, preferred_element_type=f32)
+            total = term if total is None else total + term
+        return total
+
+    def make(i):
+        slot = order[i]
+        if done_down_box[0] < i + 1:
+            done_down_box[0] += 1
+            step((2,), done_down_box[0])
+        swapped(2, i + 1)
+        pcs[i] = product(slot, pl.multiple_of(other * half, half)).astype(bf16)
+        send(pcs.at[i], pcr.at[i], pc_send.at[i], pc_recv.at[i], partner)
+        keep[i] = product(slot, pl.multiple_of(core * half, half))
+
+    def chip_rows(i, xx, side):
+        at = pl.multiple_of(lax.rem(xx + N_X, N_X) * rows, rows)
+        lanes = slice(side * width, (side + 1) * width)
+        return keep[i, pl.ds(at, rows), lanes] + pcr[i, pl.ds(at, rows), lanes].astype(f32)
+
+    def spread(i):
+        landed(pcr.at[i], pc_send.at[i], pc_recv.at[i], partner)
+        for side in range(2):
+            forth, back = ways[side]
+            sign = 1 - 2 * side
+            n = 2 * i + side
+            raws[n] = chip_rows(i, x + 2, side).astype(bf16)
+            send(raws.at[n], rawr.at[n], raw_send.at[n], raw_recv.at[n], forth)
+            nbs[n, 1] = chip_rows(i, x - sign, side).astype(bf16)
+            send(nbs.at[n, 1], nbr.at[n, 1], nb_send.at[2 * n + 1], nb_recv.at[2 * n + 1], back)
+
+    def pass_on(i):
+        for side in range(2):
+            forth, back = ways[side]
+            sign = 1 - 2 * side
+            n = 2 * i + side
+            landed(rawr.at[n], raw_send.at[n], raw_recv.at[n], back)
+            nbs[n, 0] = (chip_rows(i, x + sign, side) + rawr[n].astype(f32)).astype(bf16)
+            send(nbs.at[n, 0], nbr.at[n, 0], nb_send.at[2 * n], nb_recv.at[2 * n], forth)
+
+    def collect(i):
+        slot = order[i]
+        for side in range(2):
+            forth, back = ways[side]
+            n = 2 * i + side
+            landed(nbr.at[n, 0], nb_send.at[2 * n], nb_recv.at[2 * n], back)
+            landed(nbr.at[n, 1], nb_send.at[2 * n + 1], nb_recv.at[2 * n + 1], forth)
+            total = chip_rows(i, x, side) + nbr[n, 0].astype(f32) + nbr[n, 1].astype(f32)
+            if slot == 0:
+                origin = s if side == 0 else lax.rem(s + REACH, N_SP)
+            else:
+                origin = lax.rem(s + N_SP - slot, N_SP) if side == 0 else lax.rem(s + slot, N_SP)
+            ffn[origin] = total
+
+    done_down_box = [done_down]
+    for i in range(REACH + 3):
+        if i < REACH:
+            make(i)
+        if 0 <= i - 1 < REACH:
+            spread(i - 1)
+        if 0 <= i - 2 < REACH:
+            pass_on(i - 2)
+        if 0 <= i - 3 < REACH:
+            collect(i - 3)
+
+    squares = None
+    for n in range(N_SP):
+        v = ffn[n].astype(bf16).astype(f32)
+        part = jnp.sum(v * v, axis=-1, keepdims=True)
+        squares = part if squares is None else squares + part
+    scale = lax.rsqrt(squares / (N_SP * width) + epsilon)
+    for n in range(N_SP):
+        lanes = slice(n * width, (n + 1) * width)
+        v = ffn[n].astype(bf16).astype(f32)
+        out_ref[:, lanes] = (
+            after_ref[:, lanes].astype(f32) + 0.5 * (v * scale * gain_ref[:, lanes])
+        ).astype(bf16)
+
+    for copy in pending:
+        copy.wait_send()
+
+
+def feed_forward(normed, after, gate_weight, up_weight, down_weight, gain_after):
+    N_SP, N_TP = lax.axis_size("sp"), lax.axis_size("tp")
+    N_X, REACH = N_TP // 2, N_SP // 2
+    rows, dim = normed.shape
+    depth, hidden = gate_weight.shape
+    width = down_weight.shape[1]
+    third = hidden // 3
+    half = N_X * rows
+    total = N_TP * rows
+    vmem = pl.BlockSpec(memory_space=pltpu.VMEM)
+    dma = pltpu.SemaphoreType.DMA
+    n_z = 3 * REACH * 2 * 2 * HALVES
+    n_y = 3 * REACH * 2 * HALVES
+    return pl.pallas_call(
+        kernel,
+        out_shape=jax.ShapeDtypeStruct((rows, dim), bf16),
+        in_specs=[vmem] * 6,
+        out_specs=vmem,
+        scratch_shapes=[
+            pltpu.VMEM((3, N_SP * depth, third), bf16),
+            pltpu.VMEM((3, N_SP * depth, third), bf16),
+            pltpu.VMEM((REACH, 2, hidden, width), bf16),
+            pltpu.VMEM((total, dim), bf16),
+            pltpu.VMEM((3, total, third), bf16),
+            pltpu.VMEM((REACH, half, 2 * width), bf16),
+            pltpu.VMEM((REACH, half, 2 * width), bf16),
+            pltpu.VMEM((REACH, half, 2 * width), f32),
+            pltpu.VMEM((2 * REACH, rows, width), bf16),
+            pltpu.VMEM((2 * REACH, rows, width), bf16),
+            pltpu.VMEM((2 * REACH, 2, rows, width), bf16),
+            pltpu.VMEM((2 * REACH, 2, rows, width), bf16),
+            pltpu.VMEM((8, 128), f32),
+            pltpu.VMEM((N_SP, rows, width), f32),
+            dma((n_z,)),
+            dma((n_z,)),
+            dma((n_y,)),
+            dma((n_y,)),
+            dma((9,)),
+            dma((9,)),
+            dma((REACH,)),
+            dma((REACH,)),
+            dma((2 * REACH,)),
+            dma((2 * REACH,)),
+            dma((4 * REACH,)),
+            dma((4 * REACH,)),
+        ],
+        compiler_params=pltpu.CompilerParams(
+            collective_id=0, has_side_effects=True, vmem_limit_bytes=60 * 1024 * 1024
+        ),
+    )(normed, after, gate_weight, up_weight, down_weight, gain_after.reshape(1, -1))
+
+
+def from_everyone(shard, axis):
+    size = lax.axis_size(axis)
+    return lax.all_to_all(
+        jnp.broadcast_to(shard[None], (size, *shard.shape)), axis, 0, 0, tiled=True
+    )
+
+
+def gather_directly(shard, axis, dim):
+    pieces = jnp.moveaxis(from_everyone(shard, axis), 0, dim)
+    lengths = pieces.shape
+    return pieces.reshape(*lengths[:dim], lengths[dim] * lengths[dim + 1], *lengths[dim + 2 :])
 
 
 def per_device(
@@ -141,21 +487,9 @@
     projected = stored(projected)
     after = stored(residual.astype(jnp.float32) + rms_scaled(projected, gain_mixed))
     normed = rms_scaled(after, gain_before).astype(jnp.bfloat16)
-    full_gate, full_up, full_down = turned_gather(
-        (gate_weight, up_weight, down_weight), "sp", (0, 0, 1)
-    )
-    piece = lax.all_gather(normed, "tp", axis=0, tiled=True)
-    gate = jnp.dot(piece, full_gate, preferred_element_type=jnp.float32)
-    upward = jnp.dot(piece, full_up, preferred_element_type=jnp.float32)
-    hidden = (jax.nn.silu(gate) * upward).astype(jnp.bfloat16)
-    ffn_out = stored(
-        summed_on_arrival(
-            jnp.dot(hidden, full_down, preferred_element_type=jnp.float32).astype(jnp.bfloat16),
-            "tp",
-            0,
-        )
-    )
-    return (after + 0.5 * rms_scaled(ffn_out, gain_after)).astype(jnp.bfloat16)
+    return feed_forward(
+        normed, after.astype(jnp.bfloat16), gate_weight, up_weight, down_weight, gain_after
+    )
 
 
 def solution(mesh):

time: 349 us -> 232 us (0.66)
  waiting for transfers between devices: 172 us -> 14.8 us
  Pallas kernels: 0 us -> 116 us
  blocking collectives: 116 us -> 63.3 us
  matrix products: 22.3 us -> 4.44 us
  other arithmetic: 8.34 us -> 2.89 us
    all_gather x2 -> x0, waiting for transfers between devices: 160 us -> none  [the longest x1 128 us: turned_gather(): lax.all_gather(both, axis, axis=0, tiled=True)]
    pallas_call x0 -> x1, Pallas kernels: none -> 116 us  [feed_forward(): pl.pallas_call(kernel, out_shape=jax.ShapeDtypeStruct((rows, dim), bf16),...]
    all_to_all x1 -> x0, blocking collectives: 51.4 us -> none  [summed_on_arrival(): pieces = lax.all_to_all(split_up(shard, dim, size), axis, 0, 0, tiled=True)]
    dot_general x2 -> x0, matrix products: 17.9 us -> none  [the longest x1 11 us: per_device(): jnp.dot(hidden, full_down, preferred_element_type=jnp.float32)]
  transfers between devices with their start and end apart: 6 -> 4, of which waited for: 3 -> 1; matrix products, arithmetic and copies ran while one was open for 2% -> 1% of each run, Pallas kernels for 0% -> 0%
where the time goes in v1:
time: 232 us; the launch traced here: 231 us
  Pallas kernels  116 us (50%)
  blocking collectives  63.3 us (27%)
  waiting for transfers between devices  14.8 us (6%)
  between operations  13.7 us (6%)
  starting transfers between devices  12.1 us (5%)
  matrix products  4.44 us (2%)
  local copies, waits for them, and re-layouts  3.79 us (2%)
  other arithmetic  2.89 us (1%)
    pallas_call x1, Pallas kernels, feed_forward(): pl.pallas_call(kernel, out_shape=jax.ShapeDtypeStruct((rows, dim), bf16),...  116 us
    all_to_all x1, blocking collectives, from_everyone(): lax.all_to_all(jnp.broadcast_to(shard[None], (size, *shard.shape)), axis,...  47.2 us
    all_to_all x1, blocking collectives, per_device(): lax.all_to_all(mixed, 'tp', split_axis=0, concat_axis=1, tiled=True)  16.1 us
    all_gather x1, waiting for transfers between devices, per_device(): lax.all_gather(head_columns, 'tp', axis=0, tiled=True)  14.7 us
    ppermute x3, starting transfers between devices, passed_along(): lax.ppermute(value, axis, [(source, source + steps) for source in range(f...  12.1 us
  transfers between devices with their start and end apart: 4, of which 1 were waited for; matrix products, arithmetic and copies ran while one was open for 1% of the time, Pallas kernels for 0%

profile of v1, /device:TPU:33, one launch (start us, length us, event | category | flops | bytes accessed | tf_op | source)
XLA Modules:
  0.0 231.3 jit_solution(14883270682048559470)
XLA Ops:
  6.5 0.0 copy-start.5
  6.5 0.0 copy-start.1
  6.6 0.0 copy-start.2
  6.6 0.0 copy-start.4
  6.6 0.1 all-gather.2.cloned.1.call-start
  6.6 1.0 copy.36
  7.6 0.1 broadcast_in_dim.16
  7.7 47.2 %all_to_all.21 = bf16[16,128,128]{1,2,0:T(8,128)(2,1)} all-to-all(bf16[16,128,128]{1,2,0:T(8,128)(2,1)S(1)} %broadcast_in_dim.16), channel_id=1, replica_groups=mesh['grp'=2,'sp'=16,'tp'=8] {'sp'}, dimensions={0} | all-to-all | bytes 1048576 | tf_op jit(solution)/shard_map/all_to_all | solution.py:453
  54.9 0.1 all-gather.2.cloned.1.call-update
  54.9 0.0 copy-done.5
  55.0 5.3 %collective-permute-start.1 = (s32[128]{0:T(128)S(1)}, s32[128]{0:T(128)S(1)}, u32[]{:S(2)}, u32[]{:S(2)}) collective-permute-start(s32[128]{0:T(128)S(1)} %slice.40), channel_id=1, source_target_pairs={{0,8},{8,16},{16,24},{24,32},{32,40},{40,48},{48,56},{56,64},{64,7... | collective-permute-start | bytes 1544 | tf_op jit(solution)/shard_map/ppermute | solution.py:24
  60.3 0.0 copy-done.1
  60.3 2.2 collective-permute-start.2
  62.5 0.0 copy-done.2
  62.5 4.6 %collective-permute-start = (bf16[128,64]{0,1:T(8,128)(2,1)S(1)}, bf16[128,64]{0,1:T(8,128)(2,1)S(1)}, u32[]{:S(2)}, u32[]{:S(2)}) collective-permute-start(bf16[128,64]{0,1:T(8,128)(2,1)S(1)} %slice.36), channel_id=1, source_target_pairs={{0,8},{8,16},{16,24},{24,32},{32,40},{40,48},{48,56},{56,64},{64,7... | collective-permute-start | bytes 49160 | tf_op jit(solution)/shard_map/ppermute | solution.py:24
  67.2 0.0 copy-done.4
  67.2 0.2 reshape.161
  67.4 0.0 collective-permute-done.1
  67.5 0.0 copy-start.8
  67.5 1.0 fusion.16
  68.4 0.0 collective-permute-done.2
  68.5 0.0 collective-permute-done
  68.5 0.5 fusion.33
  69.0 0.0 copy-done.8
  69.0 0.1 broadcast_maximum_fusion
  69.1 0.2 fusion
  69.3 0.1 fusion.29
  69.4 0.4 fusion.3
  69.8 0.4 copy.42
  70.2 0.2 reshape.162
  70.4 16.1 %all_to_all.22 = bf16[8,96,128]{2,1,0:T(8,128)(2,1)S(1)} all-to-all(bf16[8,96,128]{2,1,0:T(8,128)(2,1)S(1)} %reshape.162), channel_id=1, replica_groups=mesh['grp'=2,'sp'=16,'tp'=8] {'tp'}, dimensions={0} | all-to-all | bytes 393216 | tf_op jit(solution)/shard_map/all_to_all | solution.py:481
  86.5 0.0 copy-start.3
  86.5 0.0 copy-start.6
  86.5 14.7 %all-gather.2.cloned.1.call-done = bf16[1024,2048]{0,1:T(8,128)(2,1)} async-done(((bf16[128,2048]{0,1:T(8,128)(2,1)}), bf16[1024,2048]{0,1:T(8,128)(2,1)}) %all-gather.2.cloned.1.call-update) | async-done | bytes 4194320 | tf_op jit(solution)/shard_map/all_gather | solution.py:484
  101.2 3.6 %convolution_convert_fusion = bf16[96,2048]{1,0:T(8,128)(2,1)S(1)} fusion(bf16[1024,2048]{0,1:T(8,128)(2,1)} %all-gather.2.cloned.1.call-done, bf16[8,96,128]{2,1,0:T(8,128)(2,1)S(1)} %all_to_all.22), kind=kOutput, calls=%fused_computation | convolution fusion | flops 402849792 | bytes 4784128 | tf_op jit(solution)/shard_map/dot_general | solution.py:482
  104.9 0.0 copy-start.7
  104.9 0.2 fusion.4
  105.0 0.0 copy-done.3
  105.1 0.0 copy-done.6
  105.1 0.2 fusion.7.after_ref
  105.3 0.0 copy-start
  105.3 0.2 fusion.8
  105.5 0.1 copy-done.7
  105.6 0.9 fusion.10.normed_ref
  106.5 0.0 copy-done
  106.5 116.2 %shard_map.127 = bf16[96,2048]{1,0:T(8,128)(2,1)} custom-call(bf16[96,2048]{1,0:T(8,128)(2,1)} %fusion.10.normed_ref, bf16[96,2048]{1,0:T(8,128)(2,1)} %copy-done, bf16[128,768]{1,0:T(8,128)(2,1)} %gate_ref.1, bf16[128,768]{1,0:T(8,128)(2,1)} %up_ref.1, bf16[768,128]{1,0:T(8,128)(2,1)} %down_ref.1, f32[1,2048]{1,0:T(1,128)} %bitcast.84), custom_call_target="tpu_custom_call" | custom-call | tf_op jit(solution)/shard_map/pallas_call | solution.py:412
  222.7 1.8 copy.62
  (16 shorter events, 0.1 us)
Async XLA Ops:
  6.5 48.4 %copy-start.5 = (s32[768]{0:T(1024)S(1)}, s32[768]{0:T(1024)}, u32[]{:S(2)}) copy-start(s32[768]{0:T(1024)} %param.16) | copy-start | bytes 9220
  6.5 53.7 %copy-start.1 = (bf16[768,64]{0,1:T(8,128)(2,1)S(1)}, bf16[768,64]{0,1:T(8,128)(2,1)}, u32[]{:S(2)}) copy-start(bf16[768,64]{0,1:T(8,128)(2,1)} %param.14) | copy-start | bytes 294916
  6.6 55.9 %copy-start.2 = (bf16[768,64]{0,1:T(8,128)(2,1)S(1)}, bf16[768,64]{0,1:T(8,128)(2,1)}, u32[]{:S(2)}) copy-start(bf16[768,64]{0,1:T(8,128)(2,1)} %param.15) | copy-start | bytes 294916
  6.6 60.7 %copy-start.4 = (bf16[768,128]{1,0:T(8,128)(2,1)S(1)}, bf16[768,128]{1,0:T(8,128)(2,1)}, u32[]{:S(2)}) copy-start(bf16[768,128]{1,0:T(8,128)(2,1)} %param.13) | copy-start | bytes 589828
  6.6 94.7 %all-gather.2.cloned.1.call-start = ((), (), s32[]{:S(2)}) async-start(), calls=%async_computation.2 | async-start | bytes 4718592 | tf_op jit(solution)/shard_map/all_gather | solution.py:484
  55.0 12.4 %collective-permute-start.1 = (s32[128]{0:T(128)S(1)}, s32[128]{0:T(128)S(1)}, u32[]{:S(2)}, u32[]{:S(2)}) collective-permute-start(s32[128]{0:T(128)S(1)} %slice.40), channel_id=1, source_target_pairs={{0,8},{8,16},{16,24},{24,32},{32,40},{40,48},{48,56},{56,64},{64,7... | collective-permute-start | bytes 1544 | tf_op jit(solution)/shard_map/ppermute | solution.py:24
  60.3 8.1 %collective-permute-start.2 = (bf16[128,64]{0,1:T(8,128)(2,1)S(1)}, bf16[128,64]{0,1:T(8,128)(2,1)S(1)}, u32[]{:S(2)}, u32[]{:S(2)}) collective-permute-start(bf16[128,64]{0,1:T(8,128)(2,1)S(1)} %slice.43), channel_id=1, source_target_pairs={{0,8},{8,16},{16,24},{24,32},{32,40},{40,48},{48,56},{56,64},{64,7... | collective-permute-start | bytes 49160 | tf_op jit(solution)/shard_map/ppermute | solution.py:24
  62.5 6.0 %collective-permute-start = (bf16[128,64]{0,1:T(8,128)(2,1)S(1)}, bf16[128,64]{0,1:T(8,128)(2,1)S(1)}, u32[]{:S(2)}, u32[]{:S(2)}) collective-permute-start(bf16[128,64]{0,1:T(8,128)(2,1)S(1)} %slice.36), channel_id=1, source_target_pairs={{0,8},{8,16},{16,24},{24,32},{32,40},{40,48},{48,56},{56,64},{64,7... | collective-permute-start | bytes 49160 | tf_op jit(solution)/shard_map/ppermute | solution.py:24
  67.5 1.5 copy-start.8
  86.5 18.6 %copy-start.3 = (bf16[96,2048]{1,0:T(8,128)(2,1)S(1)}, bf16[96,2048]{1,0:T(8,128)(2,1)}, u32[]{:S(2)}) copy-start(bf16[96,2048]{1,0:T(8,128)(2,1)} %param.19) | copy-start | bytes 1179652
  86.5 18.6 %copy-start.6 = (f32[2048]{0:T(1024)S(1)}, f32[2048]{0:T(1024)}, u32[]{:S(2)}) copy-start(f32[2048]{0:T(1024)} %param.20) | copy-start | bytes 24580
  104.9 0.7 copy-start.7
  105.3 1.2 copy-start
Sparse Core Ops, SparseCore 0:
  55.1 46.1 all-gather.1

commit v2 on v0

v2 whole, which is shorter than its diff:
```python
import jax
import jax.numpy as jnp
from jax import lax
from jax.experimental import pallas as pl
from jax.experimental.pallas import tpu as pltpu
from jax.sharding import PartitionSpec as P

HEAD_DIM = 64
WINDOW = 128
epsilon = 1e-06
masked_value = -1e30
MESH = pl.DeviceIdType.MESH
f32 = jnp.float32
bf16 = jnp.bfloat16

PARTS = {"gate": 2, "up": 2, "down": 2, "out": 1}
LAGS = {"out": 0, "gate": 0, "up": 4, "down": 8}


def kernel(
    query_ref,
    key_ref,
    value_ref,
    doc_ref,
    sink_ref,
    residual_ref,
    gain_mixed_ref,
    gain_before_ref,
    gain_after_ref,
    out_weight_ref,
    gate_ref,
    up_ref,
    down_ref,
    out_ref,
    keys,
    values,
    docs,
    mixed,
    heads,
    ofull,
    gfull,
    ufull,
    dfull,
    proj,
    after,
    normed,
    xn,
    hid,
    keep,
    pcs,
    pcr,
    raws,
    rawr,
    nbs,
    nbr,
    ffn,
    halo_send,
    halo_recv,
    z_send,
    z_recv,
    y_send,
    y_recv,
    ag_send,
    ag_recv,
    pc_send,
    pc_recv,
    raw_send,
    raw_recv,
    nb_send,
    nb_recv,
):
    n_sp, n_tp = lax.axis_size("sp"), lax.axis_size("tp")
    n_x, reach = n_tp // 2, n_sp // 2
    g = lax.axis_index("grp")
    s = lax.axis_index("sp")
    t = lax.axis_index("tp")
    core = lax.rem(t, 2)
    other = 1 - core
    x = t // 2
    length = query_ref.shape[0]
    rows, dim = residual_ref.shape
    half = n_x * rows
    depth = gate_ref.shape[0]
    third = gate_ref.shape[1] // 3
    width = down_ref.shape[1]

    z_next = {"sp": lax.rem(s + 1, n_sp)}
    z_prev = {"sp": lax.rem(s + n_sp - 1, n_sp)}
    z_to = (z_next, z_prev)
    x_next = {"tp": lax.rem(t + 2, n_tp)}
    x_prev = {"tp": lax.rem(t + n_tp - 2, n_tp)}
    partner = {"tp": t + 1 - 2 * core}
    odd = lax.rem(g, 2)
    y_pair = {"grp": g + 1 - 2 * odd}
    mine, theirs = 2 * odd, 2 - 2 * odd

    barrier = pltpu.get_barrier_semaphore()
    for device in (z_next, z_prev, x_next, x_prev, partner, y_pair):
        pl.semaphore_signal(barrier, inc=1, device_id=device, device_id_type=MESH)
    pl.semaphore_wait(barrier, 6)

    pending = []

    def send(src, dst, ssem, rsem, device):
        copy = pltpu.make_async_remote_copy(
            src_ref=src, dst_ref=dst, send_sem=ssem, recv_sem=rsem, device_id=device, device_id_type=MESH
        )
        copy.start()
        pending.append(copy)

    def landed(dst, ssem, rsem, device):
        pltpu.make_async_remote_copy(
            src_ref=dst, dst_ref=dst, send_sem=ssem, recv_sem=rsem, device_id=device, device_id_type=MESH
        ).wait_recv()

    fulls = {"gate": gfull, "up": ufull}
    owns = {"gate": gate_ref, "up": up_ref}
    names = ("gate", "up", "down", "out")
    z_base, y_base, z_at, y_at = {}, {}, 0, 0
    for name in names:
        z_base[name], y_base[name] = z_at, y_at
        z_at += reach * 4 * PARTS[name]
        y_at += reach * 2 * PARTS[name]

    def place(name, j, way, part, h):
        if name in fulls:
            origin = lax.rem(s + n_sp - j, n_sp) if way == 0 else lax.rem(s + j, n_sp)
            size = depth // PARTS[name]
            at = pl.multiple_of(origin * depth + h * size, size)
            return fulls[name].at[part, pl.ds(at, size), :]
        slot, side = (0, 1) if j == reach else (j, way)
        if name == "out":
            size = out_weight_ref.shape[0] // 2
            return ofull.at[slot, side, pl.ds(part * size, size), :]
        size = third // PARTS[name]
        at = pl.multiple_of(part * third + h * size, size)
        return dfull.at[slot, side, pl.ds(at, size), :]

    def dest(name, j, way, part, h):
        return place(name, j if name in fulls else j + 1, way, part, h)

    def own_piece(name, part, h):
        if name in fulls:
            size = depth // PARTS[name]
            lanes = pl.ds(pl.multiple_of(part * third, third), third)
            return owns[name].at[pl.ds(h * size, size), lanes]
        if name == "out":
            size = out_weight_ref.shape[0] // 2
            return out_weight_ref.at[pl.ds(part * size, size), :]
        size = third // PARTS[name]
        return down_ref.at[pl.ds(pl.multiple_of(part * third + h * size, size), size), :]

    def z_sem(name, j, way, kind, h):
        return z_base[name] + ((j * 2 + way) * 2 + kind) * PARTS[name] + h

    def y_sem(name, j, way, h):
        return y_base[name] + ((j - 1) * 2 + way) * PARTS[name] + h

    def travels(j, way, kind):
        return j < reach - 1 or (j == reach - 1 and way == kind)

    def part_of(name, kind):
        if name == "out":
            return kind
        return mine if kind == 0 else 1

    def start_own(name):
        for kind in range(2):
            for h in range(PARTS[name]):
                for way in range(2):
                    i = z_sem(name, 0, way, kind, h)
                    part = part_of(name, kind)
                    send(
                        own_piece(name, part, h),
                        dest(name, 0, way, part, h),
                        z_send.at[i],
                        z_recv.at[i],
                        z_to[way],
                    )

    def step(name, j):
        for kind in range(2):
            part = part_of(name, kind)
            for h in range(PARTS[name]):
                for way in range(2):
                    if not travels(j - 1, way, kind):
                        continue
                    here = place(name, j, way, part, h)
                    i = z_sem(name, j - 1, way, kind, h)
                    landed(here, z_send.at[i], z_recv.at[i], z_to[1 - way])
                    if j < reach and travels(j, way, kind):
                        k = z_sem(name, j, way, kind, h)
                        there = dest(name, j, way, part, h)
                        send(here, there, z_send.at[k], z_recv.at[k], z_to[way])
                    if kind == 0 and name != "out":
                        k = y_sem(name, j, way, h)
                        send(here, here, y_send.at[k], y_recv.at[k], y_pair)

    def turn(r):
        for name in ("out", "gate", "up", "down"):
            if 1 <= r - LAGS[name] <= reach:
                step(name, r - LAGS[name])
        for name in ("gate", "up", "down"):
            if LAGS[name] == r:
                start_own(name)

    def swapped(name, j):
        for way in range(2):
            if not travels(j - 1, way, 0):
                continue
            for h in range(PARTS[name]):
                k = y_sem(name, j, way, h)
                landed(place(name, j, way, theirs, h), y_send.at[k], y_recv.at[k], y_pair)

    order = [*range(1, reach), 0]
    ways = ((x_next, x_prev), (x_prev, x_next))

    def origin_of(slot, side):
        if slot == 0:
            return s if side == 0 else lax.rem(s + reach, n_sp)
        return lax.rem(s + n_sp - slot, n_sp) if side == 0 else lax.rem(s + slot, n_sp)

    def summing(which, product, result):
        def slot_of(i):
            return which * reach + i

        def make(i):
            m = slot_of(i)
            pcs[m] = product(order[i], pl.multiple_of(other * half, half)).astype(bf16)
            send(pcs.at[m], pcr.at[m], pc_send.at[m], pc_recv.at[m], partner)
            keep[i] = product(order[i], pl.multiple_of(core * half, half))

        def chip_rows(i, xx, side):
            at = pl.multiple_of(lax.rem(xx + n_x, n_x) * rows, rows)
            lanes = slice(side * width, (side + 1) * width)
            return keep[i, pl.ds(at, rows), lanes] + pcr[slot_of(i), pl.ds(at, rows), lanes].astype(f32)

        def spread(i):
            m = slot_of(i)
            landed(pcr.at[m], pc_send.at[m], pc_recv.at[m], partner)
            for side in range(2):
                forth, back = ways[side]
                sign = 1 - 2 * side
                n = 2 * m + side
                raws[n] = chip_rows(i, x + 2, side).astype(bf16)
                send(raws.at[n], rawr.at[n], raw_send.at[n], raw_recv.at[n], forth)
                nbs[n, 1] = chip_rows(i, x - sign, side).astype(bf16)
                send(nbs.at[n, 1], nbr.at[n, 1], nb_send.at[2 * n + 1], nb_recv.at[2 * n + 1], back)

        def pass_on(i):
            for side in range(2):
                forth, back = ways[side]
                sign = 1 - 2 * side
                n = 2 * slot_of(i) + side
                landed(rawr.at[n], raw_send.at[n], raw_recv.at[n], back)
                nbs[n, 0] = (chip_rows(i, x + sign, side) + rawr[n].astype(f32)).astype(bf16)
                send(nbs.at[n, 0], nbr.at[n, 0], nb_send.at[2 * n], nb_recv.at[2 * n], forth)

        def collect(i):
            for side in range(2):
                forth, back = ways[side]
                n = 2 * slot_of(i) + side
                landed(nbr.at[n, 0], nb_send.at[2 * n], nb_recv.at[2 * n], back)
                landed(nbr.at[n, 1], nb_send.at[2 * n + 1], nb_recv.at[2 * n + 1], forth)
                total = chip_rows(i, x, side) + nbr[n, 0].astype(f32) + nbr[n, 1].astype(f32)
                result[origin_of(order[i], side)] = total

        return make, spread, pass_on, collect

    def block_of(c, xx):
        return pl.multiple_of((c * n_x + lax.rem(xx + n_x, n_x)) * rows, rows)

    for i, (src, dst) in enumerate(((key_ref, keys), (value_ref, values))):
        send(
            src.at[pl.ds(length - WINDOW, WINDOW), :],
            dst.at[pl.ds(0, WINDOW), :],
            halo_send.at[i],
            halo_recv.at[i],
            z_next,
        )
    send(
        doc_ref.at[:, pl.ds(length - WINDOW, WINDOW)],
        docs.at[:, pl.ds(0, WINDOW)],
        halo_send.at[2],
        halo_recv.at[2],
        z_next,
    )
    for name in ("out", "gate", "up", "down"):
        if LAGS[name] == 0:
            start_own(name)
    keys[WINDOW:, :] = key_ref[...]
    values[WINDOW:, :] = value_ref[...]
    docs[:, WINDOW:] = doc_ref[...]

    def column(row):
        return jnp.transpose(jnp.broadcast_to(row, (WINDOW, WINDOW)))

    def attend(b):
        first = b * WINDOW
        query = query_ref[first : first + WINDOW, :]
        query = jnp.concatenate([query[:, :HEAD_DIM], query[:, HEAD_DIM:]], axis=0)
        window = slice(first, first + 2 * WINDOW)
        scores = lax.dot_general(
            query, keys[window, :], (((1,), (1,)), ((), ())), preferred_element_type=f32
        ) * HEAD_DIM ** (-0.5)
        at_row = lax.broadcasted_iota(jnp.int32, (WINDOW, 2 * WINDOW), 0)
        at_col = lax.broadcasted_iota(jnp.int32, (WINDOW, 2 * WINDOW), 1)
        distance = at_row - at_col + WINDOW
        place_of_key = s * length + (first - WINDOW) + at_col
        mine_doc = column(docs[:, first + WINDOW : first + 2 * WINDOW])
        mine_doc = jnp.concatenate([mine_doc, mine_doc], axis=1)
        valid = (distance >= 0) & (distance < WINDOW) & (place_of_key >= 0)
        valid = valid & (mine_doc == docs[:, window])
        bias = jnp.where(valid, 0.0, masked_value)
        bias = jnp.concatenate([bias, bias], axis=0)
        scores = jnp.where(bias < 0.0, masked_value, scores)
        head = lax.broadcasted_iota(jnp.int32, (2 * WINDOW, 1), 0)
        sinks = jnp.where(head < WINDOW, sink_ref[0], sink_ref[1])
        top = jnp.maximum(jnp.max(scores, axis=-1, keepdims=True), sinks)
        weight = jnp.exp(scores - top)
        denom = jnp.sum(weight, axis=-1, keepdims=True) + jnp.exp(sinks - top)
        summed = jnp.dot(weight.astype(bf16), values[window, :], preferred_element_type=f32) / denom
        mixed[first : first + WINDOW, :] = jnp.concatenate(
            [summed[:WINDOW], summed[WINDOW:]], axis=1
        ).astype(bf16)

    blocks = length // WINDOW
    for b in range(1, blocks):
        attend(b)
    landed(keys.at[pl.ds(0, WINDOW), :], halo_send.at[0], halo_recv.at[0], z_prev)
    landed(values.at[pl.ds(0, WINDOW), :], halo_send.at[1], halo_recv.at[1], z_prev)
    landed(docs.at[:, pl.ds(0, WINDOW)], halo_send.at[2], halo_recv.at[2], z_prev)
    attend(0)
    for d in range(n_tp):
        u = (d % 2) * n_x + d // 2
        heads[u * rows : (u + 1) * rows, :] = mixed[d * rows : (d + 1) * rows, :]
    ofull[0, 0] = out_weight_ref[...]

    def project(slot, at):
        right = jnp.concatenate([ofull[slot, side] for side in range(2)], axis=1)
        return jnp.dot(heads[pl.ds(at, half), :], right, preferred_element_type=f32)

    make, spread, pass_on, collect = summing(0, project, proj)
    for i in range(reach + 3):
        turn(i + 1)
        if i < reach:
            make(i)
        if 0 <= i - 1 < reach:
            spread(i - 1)
        if 0 <= i - 2 < reach:
            pass_on(i - 2)
        if 0 <= i - 3 < reach:
            collect(i - 3)

    for name in fulls:
        at = pl.multiple_of(s * depth, depth)
        for k in range(3):
            fulls[name][k, pl.ds(at, depth), :] = owns[name][:, k * third : (k + 1) * third]
    dfull[0, 0] = down_ref[...]

    def scale_of(squares):
        return lax.rsqrt(squares / dim + epsilon)

    squares = None
    for n in range(n_sp):
        v = proj[n].astype(bf16).astype(f32)
        part = jnp.sum(v * v, axis=-1, keepdims=True)
        squares = part if squares is None else squares + part
    scale = scale_of(squares)
    squares = None
    for n in range(n_sp):
        lanes = slice(n * width, (n + 1) * width)
        v = proj[n].astype(bf16).astype(f32)
        v = residual_ref[:, lanes].astype(f32) + v * scale * gain_mixed_ref[:, lanes]
        v = v.astype(bf16)
        after[:, lanes] = v
        v = v.astype(f32)
        part = jnp.sum(v * v, axis=-1, keepdims=True)
        squares = part if squares is None else squares + part
    scale = scale_of(squares)
    for n in range(n_sp):
        lanes = slice(n * width, (n + 1) * width)
        v = after[:, lanes].astype(f32)
        normed[:, lanes] = (v * scale * gain_before_ref[:, lanes]).astype(bf16)

    h_rows = rows // 2
    ag_at = {}

    def row_part(c, xx, h):
        return xn.at[pl.ds(pl.multiple_of(block_of(c, xx) + h * h_rows, h_rows), h_rows), :]

    def ag_send_to(key, src, dst, device):
        i = ag_at[key] = len(ag_at)
        send(src, dst, ag_send.at[i], ag_recv.at[i], device)

    def ag_wait(key, dst):
        landed(dst, ag_send.at[ag_at[key]], ag_recv.at[ag_at[key]], partner)

    for h in range(2):
        src = normed.at[pl.ds(h * h_rows, h_rows), :]
        ag_send_to(("next", h), src, row_part(core, x, h), x_next)
        src = normed.at[pl.ds((1 - h) * h_rows, h_rows), :]
        ag_send_to(("prev", 1 - h), src, row_part(core, x, 1 - h), x_prev)
        src = normed.at[pl.ds(h * h_rows, h_rows), :]
        ag_send_to(("own", h), src, row_part(core, x, h), partner)
    xn[pl.ds(block_of(core, x), rows), :] = normed[...]

    def relay(h):
        for key, hh, xx, far, to in (("next", h, x - 1, 0, x_next), ("prev", 1 - h, x + 1, 1, x_prev)):
            here = row_part(core, xx, hh)
            ag_wait((key, hh), here)
            if hh == far:
                ag_send_to(("far", hh), here, here, to)
            ag_send_to((key, hh, "partner"), here, here, partner)

    def relay_far(h):
        here = row_part(core, x + 2, h)
        ag_wait(("far", h), here)
        ag_send_to(("far", h, "partner"), here, here, partner)

    last = reach + 3
    turn(last + 1)
    relay(0)
    turn(last + 2)
    relay(1)
    turn(last + 3)
    relay_far(0)
    relay_far(1)
    for h in range(2):
        ag_wait(("own", h), row_part(other, x, h))
        ag_wait(("next", h, "partner"), row_part(other, x - 1, h))
        ag_wait(("prev", h, "partner"), row_part(other, x + 1, h))
        ag_wait(("far", h, "partner"), row_part(other, x + 2, h))

    last = max(last + 3, LAGS["gate"] + reach, LAGS["up"] + reach)
    for r in range(reach + 7, last + 1):
        turn(r)
    for j in range(1, reach + 1):
        swapped("gate", j)
    for j in range(1, reach + 1):
        swapped("up", j)

    for k in range(3):
        for b in range(2):
            piece = xn[b * half : (b + 1) * half, :]
            gate = jnp.dot(piece, gfull[k], preferred_element_type=f32)
            up = jnp.dot(piece, ufull[k], preferred_element_type=f32)
            hid[k, b * half : (b + 1) * half, :] = (gate / (1.0 + jnp.exp(-gate)) * up).astype(bf16)
            last += 1
            turn(last)

    def lower(slot, at):
        total = None
        for k in range(3):
            right = jnp.concatenate(
                [dfull[slot, side, k * third : (k + 1) * third, :] for side in range(2)], axis=1
            )
            term = jnp.dot(hid[k, pl.ds(at, half), :], right, preferred_element_type=f32)
            total = term if total is None else total + term
        return total

    make, spread, pass_on, collect = summing(1, lower, ffn)
    for i in range(reach + 3):
        while last < i + 1 + LAGS["down"] and i < reach:
            last += 1
            turn(last)
        if i < reach:
            swapped("down", i + 1)
            make(i)
        if 0 <= i - 1 < reach:
            spread(i - 1)
        if 0 <= i - 2 < reach:
            pass_on(i - 2)
        if 0 <= i - 3 < reach:
            collect(i - 3)

    squares = None
    for n in range(n_sp):
        v = ffn[n].astype(bf16).astype(f32)
        part = jnp.sum(v * v, axis=-1, keepdims=True)
        squares = part if squares is None else squares + part
    scale = scale_of(squares)
    for n in range(n_sp):
        lanes = slice(n * width, (n + 1) * width)
        v = ffn[n].astype(bf16).astype(f32)
        out_ref[:, lanes] = (
            after[:, lanes].astype(f32) + 0.5 * (v * scale * gain_after_ref[:, lanes])
        ).astype(bf16)

    for copy in pending:
        copy.wait_send()


def per_device(
    queries,
    key_rows,
    value_rows,
    doc_ids,
    sink_logits,
    out_weight,
    residual,
    gain_mixed,
    gain_before,
    gain_after,
    gate_weight,
    up_weight,
    down_weight,
):
    n_sp, n_tp = lax.axis_size("sp"), lax.axis_size("tp")
    n_x, reach = n_tp // 2, n_sp // 2
    length = queries.shape[0]
    rows, dim = residual.shape
    depth, hidden = gate_weight.shape
    width = down_weight.shape[1]
    third = hidden // 3
    half = n_x * rows
    vmem = pl.BlockSpec(memory_space=pltpu.VMEM)
    smem = pl.BlockSpec(memory_space=pltpu.SMEM)
    dma = pltpu.SemaphoreType.DMA
    pieces = sum(PARTS.values())
    return pl.pallas_call(
        kernel,
        out_shape=jax.ShapeDtypeStruct((rows, dim), bf16),
        in_specs=[vmem] * 4 + [smem] + [vmem] * 8,
        out_specs=vmem,
        scratch_shapes=[
            pltpu.VMEM((length + WINDOW, key_rows.shape[1]), bf16),
            pltpu.VMEM((length + WINDOW, value_rows.shape[1]), bf16),
            pltpu.VMEM((1, length + WINDOW), jnp.int32),
            pltpu.VMEM(queries.shape, bf16),
            pltpu.VMEM(queries.shape, bf16),
            pltpu.VMEM((reach, 2, *out_weight.shape), bf16),
            pltpu.VMEM((3, n_sp * depth, third), bf16),
            pltpu.VMEM((3, n_sp * depth, third), bf16),
            pltpu.VMEM((reach, 2, hidden, width), bf16),
            pltpu.VMEM((n_sp, rows, width), f32),
            pltpu.VMEM((rows, dim), bf16),
            pltpu.VMEM((rows, dim), bf16),
            pltpu.VMEM((length, dim), bf16),
            pltpu.VMEM((3, length, third), bf16),
            pltpu.VMEM((reach, half, 2 * width), f32),
            pltpu.VMEM((2 * reach, half, 2 * width), bf16),
            pltpu.VMEM((2 * reach, half, 2 * width), bf16),
            pltpu.VMEM((4 * reach, rows, width), bf16),
            pltpu.VMEM((4 * reach, rows, width), bf16),
            pltpu.VMEM((4 * reach, 2, rows, width), bf16),
            pltpu.VMEM((4 * reach, 2, rows, width), bf16),
            pltpu.VMEM((n_sp, rows, width), f32),
            dma((3,)),
            dma((3,)),
            dma((4 * reach * pieces,)),
            dma((4 * reach * pieces,)),
            dma((2 * reach * pieces,)),
            dma((2 * reach * pieces,)),
            dma((14,)),
            dma((14,)),
            dma((2 * reach,)),
            dma((2 * reach,)),
            dma((4 * reach,)),
            dma((4 * reach,)),
            dma((8 * reach,)),
            dma((8 * reach,)),
        ],
        compiler_params=pltpu.CompilerParams(
            collective_id=0, has_side_effects=True, vmem_limit_bytes=60 * 1024 * 1024
        ),
    )(
        queries,
        key_rows,
        value_rows,
        doc_ids.reshape(1, -1),
        sink_logits,
        residual,
        gain_mixed.reshape(1, -1),
        gain_before.reshape(1, -1),
        gain_after.reshape(1, -1),
        out_weight,
        gate_weight,
        up_weight,
        down_weight,
    )


def solution(mesh):
    return jax.shard_map(
        per_device,
        mesh=mesh,
        in_specs=(
            P(("grp", "sp"), "tp"),
            P(("grp", "sp"), "tp"),
            P(("grp", "sp"), "tp"),
            P(("grp", "sp")),
            P("tp"),
            P("tp", "sp"),
            P(("grp", "sp", "tp"), None),
            P(),
            P(),
            P(),
            P("sp", "tp"),
            P("sp", "tp"),
            P("tp", "sp"),
        ),
        out_specs=P(("grp", "sp", "tp"), None),
        check_vma=False,
    )
```

time: 349 us -> 149 us (0.43)
  waiting for transfers between devices: 172 us -> 0 us
  Pallas kernels: 0 us -> 142 us
  blocking collectives: 116 us -> 0 us
  matrix products: 22.3 us -> 0 us
  between operations: 13.5 us -> 0.01 us
  starting transfers between devices: 12.4 us -> 0 us
  other arithmetic: 8.34 us -> 0 us
    all_gather x3 -> x0, waiting for transfers between devices: 172 us -> none  [the longest x1 128 us: turned_gather(): lax.all_gather(both, axis, axis=0, tiled=True)]
    pallas_call x0 -> x1, Pallas kernels: none -> 142 us  [per_device(): pl.pallas_call(kernel, out_shape=jax.ShapeDtypeStruct((rows, dim), bf16),...]
    all_to_all x3 -> x0, blocking collectives: 116 us -> none  [the longest x1 51.4 us: summed_on_arrival(): pieces = lax.all_to_all(split_up(shard, dim, size), axis, 0, 0, tiled=True)]
    dot_general x5 -> x0, matrix products: 22.3 us -> none  [the longest x1 11 us: per_device(): jnp.dot(hidden, full_down, preferred_element_type=jnp.float32)]
    ppermute x3 -> x0, starting transfers between devices: 12 us -> none  [passed_along(): lax.ppermute(value, axis, [(source, source + steps) for source in range(f...]
    unnamed x29 -> x7, local copies, waits for them, and re-layouts: 1.34 us -> 5.01 us
  transfers between devices with their start and end apart: 6 -> 0, of which waited for: 3 -> 0; matrix products, arithmetic and copies ran while one was open for 2% -> 0% of each run, Pallas kernels for 0% -> 0%
where the time goes in v2:
time: 149 us; the launch traced here: 148 us
  Pallas kernels  142 us (95%)
  local copies, waits for them, and re-layouts  5.59 us (4%)
    pallas_call x1, Pallas kernels, per_device(): pl.pallas_call(kernel, out_shape=jax.ShapeDtypeStruct((rows, dim), bf16),...  142 us
    unnamed x7, local copies, waits for them, and re-layouts  5.01 us

profile of v2, /device:TPU:33, one launch (start us, length us, event | category | flops | bytes accessed | tf_op | source)
XLA Modules:
  0.0 147.6 jit_solution(6451814984556760617)
XLA Ops:
  0.0 0.0 copy-start.1
  0.0 0.7 copy-done.1
  0.7 0.6 reshape.12.doc_ref
  1.3 0.0 copy-start
  1.3 1.7 %copy.14.key_ref = bf16[768,64]{1,0:T(8,128)(2,1)} copy(bf16[768,64]{0,1:T(8,128)(2,1)} %param.14) | data formatting | bytes 196608 | tf_op args[1]
  3.0 0.0 copy-done
  3.0 0.8 copy.15.value_ref
  3.8 142.0 %shard_map.127 = bf16[96,2048]{1,0:T(8,128)(2,1)} custom-call(bf16[768,128]{1,0:T(8,128)(2,1)} %query_ref.1, bf16[768,64]{1,0:T(8,128)(2,1)} %copy.14.key_ref, bf16[768,64]{1,0:T(8,128)(2,1)} %copy.15.value_ref, s32[1,768]{1,0:T(1,128)} %reshape.12.doc_ref, f32[2]{0:T(128)} %sink_ref.1, bf16[96,2048]{1,0:T(8,128)(2,1)} %residual_ref.1, f32[1,2048]{1,0:T(1,128)} %bitcast.3, ...), custom_call_target="tpu_custom_call" | custom-call | tf_op jit(solution)/shard_map/pallas_call | solution.py:521
  145.9 1.8 %copy.17 = bf16[96,2048]{1,0:T(8,128)(2,1)} copy(bf16[96,2048]{1,0:T(8,128)(2,1)} %shard_map.127) | data formatting | bytes 786432
Async XLA Ops:
  0.0 0.7 copy-start.1
  1.3 1.7 %copy-start = (bf16[768,64]{0,1:T(8,128)(2,1)S(1)}, bf16[768,64]{0,1:T(8,128)(2,1)}, u32[]{:S(2)}) copy-start(bf16[768,64]{0,1:T(8,128)(2,1)} %param.15) | copy-start | bytes 294916

commit v3 on v2

v3 whole, which is shorter than its diff:
```python
import functools

import jax
import jax.numpy as jnp
from jax import lax
from jax.experimental import pallas as pl
from jax.experimental.pallas import tpu as pltpu
from jax.sharding import PartitionSpec as P

HEAD_DIM = 64
WINDOW = 128
epsilon = 1e-06
masked_value = -1e30
MESH = pl.DeviceIdType.MESH
f32 = jnp.float32
bf16 = jnp.bfloat16

PARTS = {"gate": 2, "up": 2, "down": 2, "out": 1}
STREAMS = (
    ("out", 0, 0),
    ("out", 1, 0),
    ("gate", 0, 0),
    ("gate", 1, 0),
    ("up", 0, 0),
    ("up", 1, 4),
    ("down", 0, 6),
    ("down", 1, 8),
)


def kernel(
    query_ref,
    key_ref,
    value_ref,
    doc_ref,
    sink_ref,
    residual_ref,
    gain_mixed_ref,
    gain_before_ref,
    gain_after_ref,
    out_weight_ref,
    gate_ref,
    up_ref,
    down_ref,
    out_ref,
    keys,
    values,
    docs,
    mixed,
    heads,
    ofull,
    gfull,
    ufull,
    dfull,
    proj,
    after,
    normed,
    xn,
    hid,
    keep,
    pcs,
    pcr,
    raws,
    rawr,
    nbs,
    nbr,
    ffn,
    halo_send,
    halo_recv,
    z_send,
    z_recv,
    y_send,
    y_recv,
    ag_send,
    ag_recv,
    pc_send,
    pc_recv,
    raw_send,
    raw_recv,
    nb_send,
    nb_recv,
):
    n_sp, n_tp = lax.axis_size("sp"), lax.axis_size("tp")
    n_x, reach = n_tp // 2, n_sp // 2
    g = lax.axis_index("grp")
    s = lax.axis_index("sp")
    t = lax.axis_index("tp")
    core = lax.rem(t, 2)
    other = 1 - core
    x = t // 2
    length = query_ref.shape[0]
    rows, dim = residual_ref.shape
    half = n_x * rows
    depth = gate_ref.shape[0]
    third = gate_ref.shape[1] // 3
    width = down_ref.shape[1]

    z_next = {"sp": lax.rem(s + 1, n_sp)}
    z_prev = {"sp": lax.rem(s + n_sp - 1, n_sp)}
    z_to = (z_next, z_prev)
    x_next = {"tp": lax.rem(t + 2, n_tp)}
    x_prev = {"tp": lax.rem(t + n_tp - 2, n_tp)}
    partner = {"tp": t + 1 - 2 * core}
    odd = lax.rem(g, 2)
    y_pair = {"grp": g + 1 - 2 * odd}
    mine, theirs = 2 * odd, 2 - 2 * odd

    barrier = pltpu.get_barrier_semaphore()
    for device in (z_next, z_prev, x_next, x_prev, partner, y_pair):
        pl.semaphore_signal(barrier, inc=1, device_id=device, device_id_type=MESH)
    pl.semaphore_wait(barrier, 6)

    def send(src, dst, ssem, rsem, device):
        pltpu.make_async_remote_copy(
            src_ref=src, dst_ref=dst, send_sem=ssem, recv_sem=rsem, device_id=device, device_id_type=MESH
        ).start()

    def sent(size, ssem):
        pltpu.make_async_remote_copy(
            src_ref=size, dst_ref=size, send_sem=ssem, recv_sem=ssem, device_id=partner, device_id_type=MESH
        ).wait_send()

    def landed(dst, ssem, rsem, device):
        pltpu.make_async_remote_copy(
            src_ref=dst, dst_ref=dst, send_sem=ssem, recv_sem=rsem, device_id=device, device_id_type=MESH
        ).wait_recv()

    fulls = {"gate": gfull, "up": ufull}
    owns = {"gate": gate_ref, "up": up_ref}
    names = ("gate", "up", "down", "out")
    z_base, z_at = {}, 0
    for name in names:
        z_base[name] = z_at
        z_at += reach * 2 * PARTS[name]

    def place(name, j, way, part, h):
        if name in fulls:
            origin = lax.rem(s + n_sp - j, n_sp) if way == 0 else lax.rem(s + j, n_sp)
            size = depth // PARTS[name]
            at = pl.multiple_of(origin * depth + h * size, size)
            return fulls[name].at[part, pl.ds(at, size), :]
        slot, side = (0, 1) if j == reach else (j, way)
        if name == "out":
            size = out_weight_ref.shape[0] // 2
            return ofull.at[slot, side, pl.ds(part * size, size), :]
        size = third // PARTS[name]
        at = pl.multiple_of(part * third + h * size, size)
        return dfull.at[slot, side, pl.ds(at, size), :]

    def dest(name, j, way, part, h):
        return place(name, j if name in fulls else j + 1, way, part, h)

    def own_piece(name, part, h):
        if name in fulls:
            size = depth // PARTS[name]
            lanes = pl.ds(pl.multiple_of(part * third, third), third)
            return owns[name].at[pl.ds(h * size, size), lanes]
        if name == "out":
            size = out_weight_ref.shape[0] // 2
            return out_weight_ref.at[pl.ds(part * size, size), :]
        size = third // PARTS[name]
        return down_ref.at[pl.ds(pl.multiple_of(part * third + h * size, size), size), :]

    def z_sem(name, j, kind, h):
        return z_recv.at[z_base[name] + (j * 2 + kind) * PARTS[name] + h]

    def y_sem(name, j):
        return y_recv.at[names.index(name) if name in fulls else 1 + j]

    def travels(j, way, kind):
        return j < reach - 1 or (j == reach - 1 and way == kind)

    def part_of(name, kind):
        if name == "out":
            return kind
        return mine if kind == 0 else 1

    def start_own(name, kind):
        part = part_of(name, kind)
        for h in range(PARTS[name]):
            for way in range(2):
                there = dest(name, 0, way, part, h)
                which = z_send.at[names.index(name)]
                send(own_piece(name, part, h), there, which, z_sem(name, 0, kind, h), z_to[way])

    def step(name, kind, j):
        part = part_of(name, kind)
        which = names.index(name)
        ends = [way for way in range(2) if travels(j - 1, way, kind)]
        for h in range(PARTS[name]):
            landed(as_many(name, len(ends)), z_send.at[which], z_sem(name, j - 1, kind, h), z_next)
            for way in ends:
                here = place(name, j, way, part, h)
                if j < reach and travels(j, way, kind):
                    there = dest(name, j, way, part, h)
                    send(here, there, z_send.at[which], z_sem(name, j, kind, h), z_to[way])
                if kind == 0 and name != "out":
                    send(here, here, y_send.at[which], y_sem(name, j), y_pair)

    def as_many(name, count):
        if name in fulls:
            return fulls[name].at[0, pl.ds(0, count * (depth // PARTS[name])), :]
        if name == "out":
            return ofull.at[0, 0, pl.ds(0, count * (out_weight_ref.shape[0] // 2)), :]
        return dfull.at[0, 0, pl.ds(0, count * (third // PARTS[name])), :]

    def steps_of(r):
        todo = []
        for name, kind, lag in STREAMS:
            if 1 <= r - lag <= reach:
                todo.append(functools.partial(step, name, kind, r - lag))
        for name, kind, lag in STREAMS:
            if 0 < lag == r:
                todo.append(functools.partial(start_own, name, kind))
        return todo

    rounds = max(lag for _, _, lag in STREAMS) + reach
    waiting = [(r, todo) for r in range(1, rounds + 1) for todo in steps_of(r)]

    def serve(count):
        for _ in range(min(count, len(waiting))):
            waiting.pop(0)[1]()

    def serve_through(r):
        while waiting and waiting[0][0] <= r:
            waiting.pop(0)[1]()

    def serve_until(name, j):
        while any(
            todo.func is step and todo.args[0] == name and todo.args[2] <= j for _, todo in waiting
        ):
            waiting.pop(0)[1]()

    def swapped(name, j=1):
        which = names.index(name)
        if name in fulls:
            size = fulls[name].at[0, pl.ds(0, (n_sp - 1) * depth), :]
        else:
            size = dfull.at[0, 0, pl.ds(0, (2 if j < reach else 1) * third), :]
        landed(size, y_send.at[which], y_sem(name, j), y_pair)

    order = [*range(1, reach), 0]
    ways = ((x_next, x_prev), (x_prev, x_next))

    def origin_of(slot, side):
        if slot == 0:
            return s if side == 0 else lax.rem(s + reach, n_sp)
        return lax.rem(s + n_sp - slot, n_sp) if side == 0 else lax.rem(s + slot, n_sp)

    def summing(which, product, result):
        def slot_of(i):
            return which * reach + i

        def make(i):
            m = slot_of(i)
            pcs[m] = product(order[i], pl.multiple_of(other * half, half)).astype(bf16)
            send(pcs.at[m], pcr.at[m], pc_send.at[0], pc_recv.at[i], partner)
            keep[i] = product(order[i], pl.multiple_of(core * half, half))

        def chip_rows(i, xx, side):
            at = pl.multiple_of(lax.rem(xx + n_x, n_x) * rows, rows)
            lanes = slice(side * width, (side + 1) * width)
            return keep[i, pl.ds(at, rows), lanes] + pcr[slot_of(i), pl.ds(at, rows), lanes].astype(f32)

        def spread(i):
            m = slot_of(i)
            landed(pcr.at[m], pc_send.at[0], pc_recv.at[i], partner)
            for side in range(2):
                forth, back = ways[side]
                sign = 1 - 2 * side
                raws[m, side] = chip_rows(i, x + 2, side).astype(bf16)
                send(raws.at[m, side], rawr.at[m, side], raw_send.at[0], raw_recv.at[i], forth)
                nbs[m, side, 1] = chip_rows(i, x - sign, side).astype(bf16)
                send(nbs.at[m, side, 1], nbr.at[m, side, 1], nb_send.at[0], nb_recv.at[i], back)

        def pass_on(i):
            m = slot_of(i)
            landed(rawr.at[m], raw_send.at[0], raw_recv.at[i], x_next)
            for side in range(2):
                forth, back = ways[side]
                sign = 1 - 2 * side
                nbs[m, side, 0] = (chip_rows(i, x + sign, side) + rawr[m, side].astype(f32)).astype(bf16)
                send(nbs.at[m, side, 0], nbr.at[m, side, 0], nb_send.at[0], nb_recv.at[i], forth)

        def collect(i):
            m = slot_of(i)
            landed(nbr.at[m], nb_send.at[0], nb_recv.at[i], x_next)
            for side in range(2):
                total = chip_rows(i, x, side) + nbr[m, side, 0].astype(f32)
                result[origin_of(order[i], side)] = total + nbr[m, side, 1].astype(f32)

        return make, spread, pass_on, collect

    def block_of(c, xx):
        return pl.multiple_of((c * n_x + lax.rem(xx + n_x, n_x)) * rows, rows)

    blocks = length // WINDOW
    docs[0] = doc_ref[blocks - 1 : blocks, :]
    for i, (src, dst) in enumerate(((key_ref, keys), (value_ref, values))):
        send(
            src.at[:, pl.ds(length - WINDOW, WINDOW)],
            dst.at[:, pl.ds(0, WINDOW)],
            halo_send.at[i],
            halo_recv.at[i],
            z_next,
        )
    send(docs.at[0], docs.at[1], halo_send.at[2], halo_recv.at[2], z_next)
    for name, kind, lag in STREAMS:
        if lag == 0:
            start_own(name, kind)
    keys[:, WINDOW:] = key_ref[...]
    values[:, WINDOW:] = value_ref[...]

    def column(row):
        return jnp.transpose(jnp.broadcast_to(row, (WINDOW, WINDOW)))

    def attend(b):
        first = b * WINDOW
        query = query_ref[first : first + WINDOW, :]
        query = jnp.concatenate([query[:, :HEAD_DIM], query[:, HEAD_DIM:]], axis=0)
        window = slice(first, first + 2 * WINDOW)
        scores = jnp.dot(query, keys[:, window], preferred_element_type=f32) * HEAD_DIM ** (-0.5)
        at_row = lax.broadcasted_iota(jnp.int32, (WINDOW, 2 * WINDOW), 0)
        at_col = lax.broadcasted_iota(jnp.int32, (WINDOW, 2 * WINDOW), 1)
        distance = at_row - at_col + WINDOW
        place_of_key = s * length + (first - WINDOW) + at_col
        own_doc = doc_ref[b : b + 1, :]
        mine_doc = column(own_doc)
        mine_doc = jnp.concatenate([mine_doc, mine_doc], axis=1)
        earlier = docs[1] if b == 0 else doc_ref[b - 1 : b, :]
        valid = (distance >= 0) & (distance < WINDOW) & (place_of_key >= 0)
        valid = valid & (mine_doc == jnp.concatenate([earlier, own_doc], axis=1))
        bias = jnp.where(valid, 0.0, masked_value)
        bias = jnp.concatenate([bias, bias], axis=0)
        scores = jnp.where(bias < 0.0, masked_value, scores)
        head = lax.broadcasted_iota(jnp.int32, (2 * WINDOW, 1), 0)
        sinks = jnp.where(head < WINDOW, sink_ref[0], sink_ref[1])
        top = jnp.maximum(jnp.max(scores, axis=-1, keepdims=True), sinks)
        weight = jnp.exp(scores - top)
        denom = jnp.sum(weight, axis=-1, keepdims=True) + jnp.exp(sinks - top)
        summed = lax.dot_general(
            weight.astype(bf16),
            values[:, window],
            (((1,), (1,)), ((), ())),
            preferred_element_type=f32,
        ) / denom
        mixed[first : first + WINDOW, :] = jnp.concatenate(
            [summed[:WINDOW], summed[WINDOW:]], axis=1
        ).astype(bf16)

    for b in range(1, blocks):
        attend(b)
    landed(keys.at[:, pl.ds(0, WINDOW)], halo_send.at[0], halo_recv.at[0], z_prev)
    landed(values.at[:, pl.ds(0, WINDOW)], halo_send.at[1], halo_recv.at[1], z_prev)
    landed(docs.at[1], halo_send.at[2], halo_recv.at[2], z_prev)
    attend(0)
    for d in range(n_tp):
        u = (d % 2) * n_x + d // 2
        heads[u * rows : (u + 1) * rows, :] = mixed[d * rows : (d + 1) * rows, :]
    ofull[0, 0] = out_weight_ref[...]

    def project(slot, at):
        right = jnp.concatenate([ofull[slot, side] for side in range(2)], axis=1)
        return jnp.dot(heads[pl.ds(at, half), :], right, preferred_element_type=f32)

    make, spread, pass_on, collect = summing(0, project, proj)
    for i in range(reach):
        serve_until("out", i + 1)
        make(i)
        if i >= 1:
            pass_on(i - 1)
        serve(1)
        spread(i)
        if i >= 1:
            collect(i - 1)
        serve_through(i + 1)
    serve(1)
    pass_on(reach - 1)
    serve(2)
    collect(reach - 1)

    for name in fulls:
        at = pl.multiple_of(s * depth, depth)
        for k in range(3):
            fulls[name][k, pl.ds(at, depth), :] = owns[name][:, k * third : (k + 1) * third]
    dfull[0, 0] = down_ref[...]

    def scale_of(squares):
        return lax.rsqrt(squares / dim + epsilon)

    def normalise():
        squares = None
        for n in range(n_sp):
            v = proj[n].astype(bf16).astype(f32)
            part = jnp.sum(v * v, axis=-1, keepdims=True)
            squares = part if squares is None else squares + part
        scale = scale_of(squares)
        squares = None
        for n in range(n_sp):
            lanes = slice(n * width, (n + 1) * width)
            v = proj[n].astype(bf16).astype(f32)
            v = residual_ref[:, lanes].astype(f32) + v * scale * gain_mixed_ref[:, lanes]
            v = v.astype(bf16)
            after[:, lanes] = v
            v = v.astype(f32)
            part = jnp.sum(v * v, axis=-1, keepdims=True)
            squares = part if squares is None else squares + part
        scale = scale_of(squares)
        for n in range(n_sp):
            lanes = slice(n * width, (n + 1) * width)
            v = after[:, lanes].astype(f32)
            normed[:, lanes] = (v * scale * gain_before_ref[:, lanes]).astype(bf16)

    normalise()

    h_rows = rows // 2
    ag_at = {}

    def row_part(c, xx, h):
        return xn.at[pl.ds(pl.multiple_of(block_of(c, xx) + h * h_rows, h_rows), h_rows), :]

    def ag_send_to(key, src, dst, device):
        if key not in ag_at:
            ag_at[key] = len(ag_at)
        send(src, dst, ag_send.at[0], ag_recv.at[ag_at[key]], device)

    def ag_wait(key, dst):
        landed(dst, ag_send.at[0], ag_recv.at[ag_at[key]], partner)

    for h in range(2):
        src = normed.at[pl.ds(h * h_rows, h_rows), :]
        ag_send_to(("next", h), src, row_part(core, x, h), x_next)
        src = normed.at[pl.ds((1 - h) * h_rows, h_rows), :]
        ag_send_to(("prev", 1 - h), src, row_part(core, x, 1 - h), x_prev)
        src = normed.at[pl.ds(h * h_rows, h_rows), :]
        ag_send_to("partner", src, row_part(core, x, h), partner)
    xn[pl.ds(block_of(core, x), rows), :] = normed[...]

    def relay(h):
        for key, hh, xx, far, to in (("next", h, x - 1, 0, x_next), ("prev", 1 - h, x + 1, 1, x_prev)):
            here = row_part(core, xx, hh)
            ag_wait((key, hh), here)
            if hh == far:
                ag_send_to(("far", hh), here, here, to)
            ag_send_to("partner", here, here, partner)

    def relay_far(h):
        here = row_part(core, x + 2, h)
        ag_wait(("far", h), here)
        ag_send_to("partner", here, here, partner)

    serve(4)
    relay(0)
    serve(4)
    relay(1)
    serve(4)
    relay_far(0)
    relay_far(1)
    ag_wait("partner", xn.at[pl.ds(block_of(other, 0), half), :])
    serve_until("gate", reach)
    serve_until("up", reach)
    swapped("gate")
    swapped("up")

    def units(k, b):
        piece = xn[b * half : (b + 1) * half, :]
        gate = jnp.dot(piece, gfull[k], preferred_element_type=f32)
        up = jnp.dot(piece, ufull[k], preferred_element_type=f32)
        hid[k, b * half : (b + 1) * half, :] = (gate / (1.0 + jnp.exp(-gate)) * up).astype(bf16)

    for k in range(3):
        for b in range(2):
            units(k, b)
            serve(1)

    def lower(slot, at):
        total = None
        for k in range(3):
            right = jnp.concatenate(
                [dfull[slot, side, k * third : (k + 1) * third, :] for side in range(2)], axis=1
            )
            term = jnp.dot(hid[k, pl.ds(at, half), :], right, preferred_element_type=f32)
            total = term if total is None else total + term
        return total

    make, spread, pass_on, collect = summing(1, lower, ffn)
    for i in range(reach + 7):
        if i < reach:
            serve_until("down", i + 1)
            swapped("down", i + 1)
            make(i)
        if 0 <= i - 1 < reach:
            spread(i - 1)
        if 0 <= i - 4 < reach:
            pass_on(i - 4)
        if 0 <= i - 7 < reach:
            collect(i - 7)

    def finish():
        squares = None
        for n in range(n_sp):
            v = ffn[n].astype(bf16).astype(f32)
            part = jnp.sum(v * v, axis=-1, keepdims=True)
            squares = part if squares is None else squares + part
        scale = scale_of(squares)
        for n in range(n_sp):
            lanes = slice(n * width, (n + 1) * width)
            v = ffn[n].astype(bf16).astype(f32)
            out_ref[:, lanes] = (
                after[:, lanes].astype(f32) + 0.5 * (v * scale * gain_after_ref[:, lanes])
            ).astype(bf16)

    finish()

    def drain():
        trips = n_sp - 1
        shard = gfull.at[pl.ds(0, 2), pl.ds(0, trips * depth), :]
        swap = gfull.at[0, pl.ds(0, trips * depth), :]
        for i, name in enumerate(names):
            if name == "out":
                sent(gfull.at[0, pl.ds(0, trips * depth // 2), :], z_send.at[i])
            else:
                sent(shard, z_send.at[i])
                sent(swap, y_send.at[i])
        sent(xn.at[pl.ds(0, length - rows), :], ag_send.at[0])
        sent(pcs, pc_send.at[0])
        sent(raws, raw_send.at[0])
        sent(nbs, nb_send.at[0])
        tail = pl.ds(0, WINDOW)
        sent(keys.at[:, tail], halo_send.at[0])
        sent(values.at[:, tail], halo_send.at[1])
        sent(docs.at[0], halo_send.at[2])

    drain()


def per_device(
    queries,
    key_rows,
    value_rows,
    doc_ids,
    sink_logits,
    out_weight,
    residual,
    gain_mixed,
    gain_before,
    gain_after,
    gate_weight,
    up_weight,
    down_weight,
):
    n_sp, n_tp = lax.axis_size("sp"), lax.axis_size("tp")
    n_x, reach = n_tp // 2, n_sp // 2
    length = queries.shape[0]
    rows, dim = residual.shape
    depth, hidden = gate_weight.shape
    width = down_weight.shape[1]
    third = hidden // 3
    half = n_x * rows
    vmem = pl.BlockSpec(memory_space=pltpu.VMEM)
    smem = pl.BlockSpec(memory_space=pltpu.SMEM)
    dma = pltpu.SemaphoreType.DMA
    pieces = sum(PARTS.values())
    return pl.pallas_call(
        kernel,
        out_shape=jax.ShapeDtypeStruct((rows, dim), bf16),
        in_specs=[vmem] * 4 + [smem] + [vmem] * 8,
        out_specs=vmem,
        scratch_shapes=[
            pltpu.VMEM((key_rows.shape[1], length + WINDOW), bf16),
            pltpu.VMEM((value_rows.shape[1], length + WINDOW), bf16),
            pltpu.VMEM((2, 1, WINDOW), jnp.int32),
            pltpu.VMEM(queries.shape, bf16),
            pltpu.VMEM(queries.shape, bf16),
            pltpu.VMEM((reach, 2, *out_weight.shape), bf16),
            pltpu.VMEM((3, n_sp * depth, third), bf16),
            pltpu.VMEM((3, n_sp * depth, third), bf16),
            pltpu.VMEM((reach, 2, hidden, width), bf16),
            pltpu.VMEM((n_sp, rows, width), f32),
            pltpu.VMEM((rows, dim), bf16),
            pltpu.VMEM((rows, dim), bf16),
            pltpu.VMEM((length, dim), bf16),
            pltpu.VMEM((3, length, third), bf16),
            pltpu.VMEM((reach, half, 2 * width), f32),
            pltpu.VMEM((2 * reach, half, 2 * width), bf16),
            pltpu.VMEM((2 * reach, half, 2 * width), bf16),
            pltpu.VMEM((2 * reach, 2, rows, width), bf16),
            pltpu.VMEM((2 * reach, 2, rows, width), bf16),
            pltpu.VMEM((2 * reach, 2, 2, rows, width), bf16),
            pltpu.VMEM((2 * reach, 2, 2, rows, width), bf16),
            pltpu.VMEM((n_sp, rows, width), f32),
            dma((3,)),
            dma((3,)),
            dma((4,)),
            dma((2 * reach * pieces,)),
            dma((3,)),
            dma((2 + reach,)),
            dma((1,)),
            dma((7,)),
            dma((1,)),
            dma((reach,)),
            dma((1,)),
            dma((reach,)),
            dma((1,)),
            dma((reach,)),
        ],
        compiler_params=pltpu.CompilerParams(
            collective_id=0, has_side_effects=True, vmem_limit_bytes=60 * 1024 * 1024
        ),
    )(
        queries,
        key_rows.T,
        value_rows.T,
        doc_ids.reshape(-1, WINDOW),
        sink_logits,
        residual,
        gain_mixed.reshape(1, -1),
        gain_before.reshape(1, -1),
        gain_after.reshape(1, -1),
        out_weight,
        gate_weight,
        up_weight,
        down_weight,
    )


def solution(mesh):
    return jax.shard_map(
        per_device,
        mesh=mesh,
        in_specs=(
            P(("grp", "sp"), "tp"),
            P(("grp", "sp"), "tp"),
            P(("grp", "sp"), "tp"),
            P(("grp", "sp")),
            P("tp"),
            P("tp", "sp"),
            P(("grp", "sp", "tp"), None),
            P(),
            P(),
            P(),
            P("sp", "tp"),
            P("sp", "tp"),
            P("tp", "sp"),
        ),
        out_specs=P(("grp", "sp", "tp"), None),
        check_vma=False,
    )
```

time: 149 us -> 135 us (0.906)
  Pallas kernels: 142 us -> 133 us
  local copies, waits for them, and re-layouts: 5.59 us -> 1.77 us
    pallas_call x1, Pallas kernels: 142 us -> 133 us  [per_device(): pl.pallas_call(kernel, out_shape=jax.ShapeDtypeStruct((rows, dim), bf16),...]
    unnamed x7 -> x1, local copies, waits for them, and re-layouts: 5.01 us -> 1.77 us
where the time goes in v3:
time: 135 us
  Pallas kernels  133 us (99%)
  local copies, waits for them, and re-layouts  1.77 us (1%)
    pallas_call x1, Pallas kernels, per_device(): pl.pallas_call(kernel, out_shape=jax.ShapeDtypeStruct((rows, dim), bf16),...  133 us

profile of v3, /device:TPU:33, one launch (start us, length us, event | category | flops | bytes accessed | tf_op | source)
XLA Modules:
  0.0 134.8 jit_solution(848705990516728008)
XLA Ops:
  0.0 133.0 %shard_map.127 = bf16[96,2048]{1,0:T(8,128)(2,1)} custom-call(bf16[768,128]{1,0:T(8,128)(2,1)} %query_ref.1, bf16[64,768]{1,0:T(8,128)(2,1)} %bitcast.6, bf16[64,768]{1,0:T(8,128)(2,1)} %bitcast.7, s32[6,128]{1,0:T(8,128)} %bitcast.11, f32[2]{0:T(128)} %sink_ref.1, bf16[96,2048]{1,0:T(8,128)(2,1)} %residual_ref.1, f32[1,2048]{1,0:T(1,128)} %bitcast.8, ...), custom_call_target="tpu_custom_call" | custom-call | tf_op jit(solution)/shard_map/pallas_call | solution.py:564
  133.0 1.8 %copy.15 = bf16[96,2048]{1,0:T(8,128)(2,1)} copy(bf16[96,2048]{1,0:T(8,128)(2,1)} %shard_map.127) | data formatting | bytes 786432

commit v4 on v3

--- a/solution.py
+++ b/solution.py
@@ -20,12 +20,15 @@
     ("out", 0, 0),
     ("out", 1, 0),
     ("gate", 0, 0),
-    ("gate", 1, 0),
+    ("gate", 1, 4),
     ("up", 0, 0),
-    ("up", 1, 4),
-    ("down", 0, 6),
-    ("down", 1, 8),
+    ("up", 1, 5),
+    ("down", 0, 7),
+    ("down", 1, 7),
 )
+SERVE_RS = (2, 2, 1)
+SERVE_AG = (5, 3, 3, 2)
+SERVE_UNITS = 1
 
 
 def kernel(
@@ -34,7 +37,7 @@
     value_ref,
     doc_ref,
     sink_ref,
-    residual_ref,
+    residual_hbm,
     gain_mixed_ref,
     gain_before_ref,
     gain_after_ref,
@@ -65,6 +68,8 @@
     nbs,
     nbr,
     ffn,
+    residual_ref,
+    own_sem,
     halo_send,
     halo_recv,
     z_send,
@@ -89,7 +94,7 @@
     other = 1 - core
     x = t // 2
     length = query_ref.shape[0]
-    rows, dim = residual_ref.shape
+    rows, dim = residual_hbm.shape
     half = n_x * rows
     depth = gate_ref.shape[0]
     third = gate_ref.shape[1] // 3
@@ -225,9 +230,10 @@
         while waiting and waiting[0][0] <= r:
             waiting.pop(0)[1]()
 
-    def serve_until(name, j):
+    def serve_until(name, j, kind=1):
         while any(
-            todo.func is step and todo.args[0] == name and todo.args[2] <= j for _, todo in waiting
+            todo.func is step and todo.args[0] == name and todo.args[1] <= kind and todo.args[2] <= j
+            for _, todo in waiting
         ):
             waiting.pop(0)[1]()
 
@@ -308,6 +314,14 @@
     for name, kind, lag in STREAMS:
         if lag == 0:
             start_own(name, kind)
+    for name in fulls:
+        at = pl.multiple_of(s * depth, depth)
+        for k in range(3):
+            mine_rows = fulls[name].at[k, pl.ds(at, depth), :]
+            pltpu.make_async_copy(owns[name].at[:, pl.ds(k * third, third)], mine_rows, own_sem.at[0]).start()
+    pltpu.make_async_copy(down_ref, dfull.at[0, 0], own_sem.at[0]).start()
+    pltpu.make_async_copy(out_weight_ref, ofull.at[0, 0], own_sem.at[0]).start()
+    pltpu.make_async_copy(residual_hbm, residual_ref, own_sem.at[1]).start()
     keys[:, WINDOW:] = key_ref[...]
     values[:, WINDOW:] = value_ref[...]
 
@@ -350,6 +364,7 @@
 
     for b in range(1, blocks):
         attend(b)
+    serve_until("out", 1)
     landed(keys.at[:, pl.ds(0, WINDOW)], halo_send.at[0], halo_recv.at[0], z_prev)
     landed(values.at[:, pl.ds(0, WINDOW)], halo_send.at[1], halo_recv.at[1], z_prev)
     landed(docs.at[1], halo_send.at[2], halo_recv.at[2], z_prev)
@@ -357,7 +372,9 @@
     for d in range(n_tp):
         u = (d % 2) * n_x + d // 2
         heads[u * rows : (u + 1) * rows, :] = mixed[d * rows : (d + 1) * rows, :]
-    ofull[0, 0] = out_weight_ref[...]
+    arrived = gfull.at[0, pl.ds(0, 9 * depth + depth // 2), :]
+    pltpu.make_async_copy(arrived, arrived, own_sem.at[0]).wait()
+    pltpu.make_async_copy(residual_hbm, residual_ref, own_sem.at[1]).wait()
 
     def project(slot, at):
         right = jnp.concatenate([ofull[slot, side] for side in range(2)], axis=1)
@@ -369,21 +386,17 @@
         make(i)
         if i >= 1:
             pass_on(i - 1)
-        serve(1)
+        if i >= 2:
+            collect(i - 2)
+        serve(SERVE_RS[2] if i == reach - 1 else 1)
         spread(i)
-        if i >= 1:
-            collect(i - 1)
-        serve_through(i + 1)
-    serve(1)
+        if i < reach - 1:
+            serve_through(i + 1)
+    serve(SERVE_RS[0])
     pass_on(reach - 1)
-    serve(2)
+    collect(reach - 2)
+    serve(SERVE_RS[1])
     collect(reach - 1)
-
-    for name in fulls:
-        at = pl.multiple_of(s * depth, depth)
-        for k in range(3):
-            fulls[name][k, pl.ds(at, depth), :] = owns[name][:, k * third : (k + 1) * third]
-    dfull[0, 0] = down_ref[...]
 
     def scale_of(squares):
         return lax.rsqrt(squares / dim + epsilon)
@@ -449,18 +462,15 @@
         ag_wait(("far", h), here)
         ag_send_to("partner", here, here, partner)
 
-    serve(4)
+    serve(SERVE_AG[0])
     relay(0)
-    serve(4)
+    serve(SERVE_AG[1])
     relay(1)
-    serve(4)
+    serve(SERVE_AG[2])
     relay_far(0)
     relay_far(1)
+    serve(SERVE_AG[3])
     ag_wait("partner", xn.at[pl.ds(block_of(other, 0), half), :])
-    serve_until("gate", reach)
-    serve_until("up", reach)
-    swapped("gate")
-    swapped("up")
 
     def units(k, b):
         piece = xn[b * half : (b + 1) * half, :]
@@ -468,10 +478,15 @@
         up = jnp.dot(piece, ufull[k], preferred_element_type=f32)
         hid[k, b * half : (b + 1) * half, :] = (gate / (1.0 + jnp.exp(-gate)) * up).astype(bf16)
 
-    for k in range(3):
+    for turn, k in enumerate((mine, theirs, 1)):
+        for name in fulls:
+            if turn == 1:
+                swapped(name)
+            else:
+                serve_until(name, reach, turn // 2)
         for b in range(2):
             units(k, b)
-            serve(1)
+            serve(SERVE_UNITS)
 
     def lower(slot, at):
         total = None
@@ -484,17 +499,26 @@
         return total
 
     make, spread, pass_on, collect = summing(1, lower, ffn)
-    for i in range(reach + 7):
-        if i < reach:
-            serve_until("down", i + 1)
-            swapped("down", i + 1)
-            make(i)
-        if 0 <= i - 1 < reach:
+    for i in range(reach):
+        if i >= 1:
             spread(i - 1)
-        if 0 <= i - 4 < reach:
-            pass_on(i - 4)
-        if 0 <= i - 7 < reach:
-            collect(i - 7)
+        if i >= 3:
+            pass_on(i - 3)
+        if i >= 5:
+            collect(i - 5)
+        serve_until("down", i + 1)
+        swapped("down", i + 1)
+        make(i)
+        serve(1)
+    pass_on(reach - 3)
+    collect(reach - 5)
+    spread(reach - 1)
+    pass_on(reach - 2)
+    collect(reach - 4)
+    collect(reach - 3)
+    pass_on(reach - 1)
+    collect(reach - 2)
+    collect(reach - 1)
 
     def finish():
         squares = None
@@ -559,12 +583,13 @@
     half = n_x * rows
     vmem = pl.BlockSpec(memory_space=pltpu.VMEM)
     smem = pl.BlockSpec(memory_space=pltpu.SMEM)
+    hbm = pl.BlockSpec(memory_space=pl.ANY)
     dma = pltpu.SemaphoreType.DMA
     pieces = sum(PARTS.values())
     return pl.pallas_call(
         kernel,
         out_shape=jax.ShapeDtypeStruct((rows, dim), bf16),
-        in_specs=[vmem] * 4 + [smem] + [vmem] * 8,
+        in_specs=[vmem] * 4 + [smem, hbm] + [vmem] * 3 + [hbm] * 4,
         out_specs=vmem,
         scratch_shapes=[
             pltpu.VMEM((key_rows.shape[1], length + WINDOW), bf16),
@@ -589,6 +614,8 @@
             pltpu.VMEM((2 * reach, 2, 2, rows, width), bf16),
             pltpu.VMEM((2 * reach, 2, 2, rows, width), bf16),
             pltpu.VMEM((n_sp, rows, width), f32),
+            pltpu.VMEM((rows, dim), bf16),
+            dma((2,)),
             dma((3,)),
             dma((3,)),
             dma((4,)),

time: 135 us -> 126 us (0.933)
  Pallas kernels: 133 us -> 123 us
    pallas_call x1, Pallas kernels: 133 us -> 123 us  [per_device(): pl.pallas_call(kernel, out_shape=jax.ShapeDtypeStruct((rows, dim), bf16),...]
where the time goes in v4:
time: 126 us; the launch traced here: 125 us
  Pallas kernels  123 us (98%)
  local copies, waits for them, and re-layouts  1.77 us (1%)
    pallas_call x1, Pallas kernels, per_device(): pl.pallas_call(kernel, out_shape=jax.ShapeDtypeStruct((rows, dim), bf16),...  123 us

profile of v4, /device:TPU:33, one launch (start us, length us, event | category | flops | bytes accessed | tf_op | source)
XLA Modules:
  0.0 125.1 jit_solution(1637176218885081158)
XLA Ops:
  0.0 123.3 %shard_map.127 = bf16[96,2048]{1,0:T(8,128)(2,1)} custom-call(bf16[768,128]{1,0:T(8,128)(2,1)} %query_ref.1, bf16[64,768]{1,0:T(8,128)(2,1)} %bitcast.6, bf16[64,768]{1,0:T(8,128)(2,1)} %bitcast.7, s32[6,128]{1,0:T(8,128)} %bitcast.11, f32[2]{0:T(128)} %sink_ref.1, bf16[96,2048]{1,0:T(8,128)(2,1)} %residual_hbm.1, f32[1,2048]{1,0:T(1,128)} %bitcast.8, ...), custom_call_target="tpu_custom_call" | custom-call | tf_op jit(solution)/shard_map/pallas_call | solution.py:589
  123.3 1.8 %copy.15 = bf16[96,2048]{1,0:T(8,128)(2,1)} copy(bf16[96,2048]{1,0:T(8,128)(2,1)} %shard_map.127) | data formatting | bytes 786432

commit v5 on v4

--- a/solution.py
+++ b/solution.py
@@ -32,15 +32,15 @@
 
 
 def kernel(
-    query_ref,
-    key_ref,
-    value_ref,
-    doc_ref,
-    sink_ref,
+    query_hbm,
+    key_hbm,
+    value_hbm,
+    doc_hbm,
+    sink_hbm,
     residual_hbm,
-    gain_mixed_ref,
-    gain_before_ref,
-    gain_after_ref,
+    gain_mixed_hbm,
+    gain_before_hbm,
+    gain_after_hbm,
     out_weight_ref,
     gate_ref,
     up_ref,
@@ -69,6 +69,12 @@
     nbr,
     ffn,
     residual_ref,
+    query_ref,
+    doc_ref,
+    sink_ref,
+    gain_mixed_ref,
+    gain_before_ref,
+    gain_after_ref,
     own_sem,
     halo_send,
     halo_recv,
@@ -93,7 +99,7 @@
     core = lax.rem(t, 2)
     other = 1 - core
     x = t // 2
-    length = query_ref.shape[0]
+    length = query_hbm.shape[0]
     rows, dim = residual_hbm.shape
     half = n_x * rows
     depth = gate_ref.shape[0]
@@ -110,9 +116,27 @@
     y_pair = {"grp": g + 1 - 2 * odd}
     mine, theirs = 2 * odd, 2 - 2 * odd
 
+    fetches = {
+        "query": (query_hbm, query_ref),
+        "key": (key_hbm, keys.at[:, pl.ds(WINDOW, length)]),
+        "value": (value_hbm, values.at[:, pl.ds(WINDOW, length)]),
+        "doc": (doc_hbm, doc_ref),
+        "sink": (sink_hbm, sink_ref),
+        "residual": (residual_hbm, residual_ref),
+        "gain_mixed": (gain_mixed_hbm, gain_mixed_ref),
+        "gain_before": (gain_before_hbm, gain_before_ref),
+        "gain_after": (gain_after_hbm, gain_after_ref),
+    }
+
+    def fetch(name):
+        src, dst = fetches[name]
+        return pltpu.make_async_copy(src, dst, own_sem.at[1 + list(fetches).index(name)])
+
     barrier = pltpu.get_barrier_semaphore()
     for device in (z_next, z_prev, x_next, x_prev, partner, y_pair):
         pl.semaphore_signal(barrier, inc=1, device_id=device, device_id_type=MESH)
+    for name in fetches:
+        fetch(name).start()
     pl.semaphore_wait(barrier, 6)
 
     def send(src, dst, ssem, rsem, device):
@@ -301,8 +325,7 @@
         return pl.multiple_of((c * n_x + lax.rem(xx + n_x, n_x)) * rows, rows)
 
     blocks = length // WINDOW
-    docs[0] = doc_ref[blocks - 1 : blocks, :]
-    for i, (src, dst) in enumerate(((key_ref, keys), (value_ref, values))):
+    for i, (src, dst) in enumerate(((key_hbm, keys), (value_hbm, values))):
         send(
             src.at[:, pl.ds(length - WINDOW, WINDOW)],
             dst.at[:, pl.ds(0, WINDOW)],
@@ -310,9 +333,14 @@
             halo_recv.at[i],
             z_next,
         )
+    for name, kind, lag in STREAMS:
+        if lag == 0 and name == "out":
+            start_own(name, kind)
+    fetch("doc").wait()
+    docs[0] = doc_ref[blocks - 1 : blocks, :]
     send(docs.at[0], docs.at[1], halo_send.at[2], halo_recv.at[2], z_next)
     for name, kind, lag in STREAMS:
-        if lag == 0:
+        if lag == 0 and name != "out":
             start_own(name, kind)
     for name in fulls:
         at = pl.multiple_of(s * depth, depth)
@@ -321,9 +349,8 @@
             pltpu.make_async_copy(owns[name].at[:, pl.ds(k * third, third)], mine_rows, own_sem.at[0]).start()
     pltpu.make_async_copy(down_ref, dfull.at[0, 0], own_sem.at[0]).start()
     pltpu.make_async_copy(out_weight_ref, ofull.at[0, 0], own_sem.at[0]).start()
-    pltpu.make_async_copy(residual_hbm, residual_ref, own_sem.at[1]).start()
-    keys[:, WINDOW:] = key_ref[...]
-    values[:, WINDOW:] = value_ref[...]
+    for name in ("query", "key", "value", "sink"):
+        fetch(name).wait()
 
     def column(row):
         return jnp.transpose(jnp.broadcast_to(row, (WINDOW, WINDOW)))
@@ -374,7 +401,8 @@
         heads[u * rows : (u + 1) * rows, :] = mixed[d * rows : (d + 1) * rows, :]
     arrived = gfull.at[0, pl.ds(0, 9 * depth + depth // 2), :]
     pltpu.make_async_copy(arrived, arrived, own_sem.at[0]).wait()
-    pltpu.make_async_copy(residual_hbm, residual_ref, own_sem.at[1]).wait()
+    for name in ("residual", "gain_mixed", "gain_before", "gain_after"):
+        fetch(name).wait()
 
     def project(slot, at):
         right = jnp.concatenate([ofull[slot, side] for side in range(2)], axis=1)
@@ -582,14 +610,13 @@
     third = hidden // 3
     half = n_x * rows
     vmem = pl.BlockSpec(memory_space=pltpu.VMEM)
-    smem = pl.BlockSpec(memory_space=pltpu.SMEM)
-    hbm = pl.BlockSpec(memory_space=pl.ANY)
+    hbm = pl.BlockSpec(memory_space=pltpu.HBM)
     dma = pltpu.SemaphoreType.DMA
     pieces = sum(PARTS.values())
     return pl.pallas_call(
         kernel,
         out_shape=jax.ShapeDtypeStruct((rows, dim), bf16),
-        in_specs=[vmem] * 4 + [smem, hbm] + [vmem] * 3 + [hbm] * 4,
+        in_specs=[hbm] * 13,
         out_specs=vmem,
         scratch_shapes=[
             pltpu.VMEM((key_rows.shape[1], length + WINDOW), bf16),
@@ -615,7 +642,13 @@
             pltpu.VMEM((2 * reach, 2, 2, rows, width), bf16),
             pltpu.VMEM((n_sp, rows, width), f32),
             pltpu.VMEM((rows, dim), bf16),
-            dma((2,)),
+            pltpu.VMEM(queries.shape, bf16),
+            pltpu.VMEM((length // WINDOW, WINDOW), jnp.int32),
+            pltpu.SMEM(sink_logits.shape, f32),
+            pltpu.VMEM((1, dim), f32),
+            pltpu.VMEM((1, dim), f32),
+            pltpu.VMEM((1, dim), f32),
+            dma((10,)),
             dma((3,)),
             dma((3,)),
             dma((4,)),
@@ -632,22 +665,27 @@
             dma((reach,)),
         ],
         compiler_params=pltpu.CompilerParams(
-            collective_id=0, has_side_effects=True, vmem_limit_bytes=60 * 1024 * 1024
+            collective_id=0, has_side_effects=True, vmem_limit_bytes=44 * 1024 * 1024
         ),
     )(
-        queries,
-        key_rows.T,
-        value_rows.T,
-        doc_ids.reshape(-1, WINDOW),
-        sink_logits,
-        residual,
-        gain_mixed.reshape(1, -1),
-        gain_before.reshape(1, -1),
-        gain_after.reshape(1, -1),
-        out_weight,
-        gate_weight,
-        up_weight,
-        down_weight,
+        *(
+            pltpu.with_memory_space_constraint(array, pltpu.HBM)
+            for array in (
+                queries,
+                key_rows.T,
+                value_rows.T,
+                doc_ids.reshape(-1, WINDOW),
+                sink_logits,
+                residual,
+                gain_mixed.reshape(1, -1),
+                gain_before.reshape(1, -1),
+                gain_after.reshape(1, -1),
+                out_weight,
+                gate_weight,
+                up_weight,
+                down_weight,
+            )
+        )
     )
 
 

time: 126 us -> 123 us (0.976)
    pallas_call x1, Pallas kernels: 123 us -> 122 us  [per_device(): pl.pallas_call(kernel, out_shape=jax.ShapeDtypeStruct((rows, dim), bf16),...]
where the time goes in v5:
time: 123 us
  Pallas kernels  122 us (99%)
    pallas_call x1, Pallas kernels, per_device(): pl.pallas_call(kernel, out_shape=jax.ShapeDtypeStruct((rows, dim), bf16),...  122 us

profile of v5, /device:TPU:33, one launch (start us, length us, event | category | flops | bytes accessed | tf_op | source)
XLA Modules:
  0.0 122.5 jit_solution(7681990563514617028)
XLA Ops:
  0.0 121.8 %shard_map.127 = bf16[96,2048]{1,0:T(8,128)(2,1)S(1)} custom-call(bf16[768,128]{1,0:T(8,128)(2,1)} %query_hbm.1, bf16[64,768]{1,0:T(8,128)(2,1)} %bitcast.6, bf16[64,768]{1,0:T(8,128)(2,1)} %bitcast.7, s32[6,128]{1,0:T(8,128)} %bitcast.11, f32[2]{0:T(128)} %sink_hbm.1, bf16[96,2048]{1,0:T(8,128)(2,1)} %residual_hbm.1, f32[1,2048]{1,0:T(1,128)} %bitcast.8, ...), custom_call_target="tpu_custom_call" | custom-call | tf_op jit(solution)/shard_map/pallas_call | solution.py:616
  121.8 0.7 copy.15

commit v6 on v5

--- a/solution.py
+++ b/solution.py
@@ -537,7 +537,8 @@
         serve_until("down", i + 1)
         swapped("down", i + 1)
         make(i)
-        serve(1)
+        if i >= 1:
+            serve(1)
     pass_on(reach - 3)
     collect(reach - 5)
     spread(reach - 1)

time: 123 us -> 123 us (level)
  no operation moved by 1% of the time
where the time goes in v6:
time: 123 us; the launch traced here: 122 us
  Pallas kernels  121 us (98%)
    pallas_call x1, Pallas kernels, per_device(): pl.pallas_call(kernel, out_shape=jax.ShapeDtypeStruct((rows, dim), bf16),...  121 us

profile of v6, /device:TPU:33, one launch (start us, length us, event | category | flops | bytes accessed | tf_op | source)
XLA Modules:
  0.0 121.9 jit_solution(3094950426823655079)
XLA Ops:
  0.0 121.1 %shard_map.127 = bf16[96,2048]{1,0:T(8,128)(2,1)S(1)} custom-call(bf16[768,128]{1,0:T(8,128)(2,1)} %query_hbm.1, bf16[64,768]{1,0:T(8,128)(2,1)} %bitcast.6, bf16[64,768]{1,0:T(8,128)(2,1)} %bitcast.7, s32[6,128]{1,0:T(8,128)} %bitcast.11, f32[2]{0:T(128)} %sink_hbm.1, bf16[96,2048]{1,0:T(8,128)(2,1)} %residual_hbm.1, f32[1,2048]{1,0:T(1,128)} %bitcast.8, ...), custom_call_target="tpu_custom_call" | custom-call | tf_op jit(solution)/shard_map/pallas_call | solution.py:617
  121.1 0.7 copy.15
